TPU v7x, 32 devices: a whole 2x2x4 slice. The times are simulated.
32 devices in a mesh: sp: 4 (over x, core), dp: 8 (over z, y).
Axes of the slice: x: 2, y: 2, z: 4, core: 2. Of those that a mesh axis runs over, the one named last changes fastest.
Arguments:
- query: bfloat16 [8, 512, 1024], P('dp', None, 'sp'), may hold values from -120 to 120
- keys: bfloat16 [8, 512, 1024], P('dp', None, 'sp'), may hold values from -6 to 6
- values: bfloat16 [8, 512, 1024], P('dp', None, 'sp'), may hold values from -6 to 6
- output: bfloat16 [8, 512, 1024], P('dp'), may hold values from -1 to 1
- cum: float32 [8, 16, 512], P('dp', 'sp'), as said below
- d_out: bfloat16 [8, 512, 2048], P('dp', 'sp'), may hold values from -6 to 6
- w_out: bfloat16 [1024, 2048], P('dp'), may hold values from -0.125 to 0.125
Outputs:
- d_query: bfloat16 [8, 512, 1024], P('dp', 'sp')
- d_key: bfloat16 [8, 512, 1024], P('dp', 'sp')
- d_value: bfloat16 [8, 512, 1024], P('dp', 'sp')
- d_cum: float32 [8, 16, 512], P('dp', 'sp')
- d_w_out: float32 [1024, 2048], P('dp', 'sp')
Inputs may be any that keep to these rules, and one draw needn't show every extreme that they name: cum never rises along positions.
All inputs are finite; a program needn't handle non-finite values.
Results may differ from a plain program's by a relative error of at most 0.008.
Values may be sent and summed in bfloat16 or wider, within the bound.
A program may use at most 64 MiB of HBM per device.

v0:
```python
import functools

import jax
import jax.numpy as jnp
from jax import lax
from jax.experimental import pallas as pl
from jax.experimental.pallas import tpu as pltpu
from jax.sharding import PartitionSpec as P


def head_grads(query, keys, values, output, cotangent, cum):
    head_count, length, head_width = query.shape
    span_rows = min(512, length)
    score_scale = head_width ** (-0.5)
    row_dots = jnp.sum(cotangent.astype(jnp.float32) * output.astype(jnp.float32), axis=2)
    positions = jnp.arange(length)

    def product(left, right, form):
        return jnp.einsum(form, left, right, preferred_element_type=jnp.float32)

    def advance(totals, block_index):
        key_grad, value_grad, cum_grad = totals
        offset = block_index * span_rows
        query_blk = lax.dynamic_slice_in_dim(query, offset, span_rows, 1)
        cot_blk = lax.dynamic_slice_in_dim(cotangent, offset, span_rows, 1)
        cum_blk = lax.dynamic_slice_in_dim(cum, offset, span_rows, 1)
        dots_blk = lax.dynamic_slice_in_dim(row_dots, offset, span_rows, 1)
        scores = product(query_blk, keys, "hqe,hke->hqk") * score_scale
        scores = scores + cum_blk[:, :, None] - cum[:, None, :]
        query_pos = offset + jnp.arange(span_rows)
        causal = positions[None, :] <= query_pos[:, None]
        scores = jnp.where(causal[None], scores, -1e30)
        row_max = jnp.max(scores, axis=2, keepdims=True)
        weights = jnp.exp(scores - row_max)
        weights = weights / jnp.sum(weights, axis=2, keepdims=True)
        weights_b = weights.astype(jnp.bfloat16)
        d_prob = product(cot_blk, values, "hqe,hke->hqk")
        d_score = weights * (d_prob - dots_blk[:, :, None])
        score_b = d_score.astype(jnp.bfloat16)
        query_grad = (product(score_b, keys, "hqk,hke->hqe") * score_scale).astype(jnp.bfloat16)
        key_grad = key_grad + product(score_b, query_blk, "hqk,hqe->hke") * score_scale
        value_grad = value_grad + product(weights_b, cot_blk, "hqk,hqe->hke")
        cum_grad = cum_grad - jnp.sum(d_score, axis=1)
        own_part = lax.dynamic_slice_in_dim(cum_grad, offset, span_rows, 1) + jnp.sum(
            d_score, axis=2
        )
        cum_grad = lax.dynamic_update_slice_in_dim(cum_grad, own_part, offset, 1)
        return ((key_grad, value_grad, cum_grad), query_grad)

    start_state = (
        jnp.zeros(query.shape, jnp.float32),
        jnp.zeros(query.shape, jnp.float32),
        jnp.zeros(cum.shape, jnp.float32),
    )
    totals, query_blocks = lax.scan(advance, start_state, jnp.arange(length // span_rows))
    query_grad = jnp.transpose(query_blocks, (1, 0, 2, 3)).reshape(query.shape)
    return (query_grad, totals[0].astype(jnp.bfloat16), totals[1].astype(jnp.bfloat16), totals[2])


def shards(query, keys, values, output, cum, d_out, w_out):
    local_rows = d_out[0]
    whole_output = output[0]
    d_attn = lax.dot_general(
        local_rows,
        lax.all_gather(w_out, "dp", axis=0, tiled=True),
        (((1,), (1,)), ((), ())),
        preferred_element_type=jnp.float32,
    ).astype(jnp.bfloat16)
    head_cot, column_part = (
        lax.all_to_all(d_attn[None], "sp", split_axis=2, concat_axis=1, tiled=True),
        lax.all_to_all(d_out, "sp", split_axis=2, concat_axis=1, tiled=True),
    )
    grad_weight = lax.psum_scatter(
        lax.dot_general(
            whole_output,
            column_part[0],
            (((0,), (0,)), ((), ())),
            preferred_element_type=jnp.float32,
        ),
        "dp",
        scatter_dimension=0,
        tiled=True,
    )
    head_cols = query.shape[2]
    head_count = cum.shape[1]
    head_width = head_cols // head_count
    seq_length = query.shape[1]
    own_output = lax.dynamic_slice_in_dim(
        whole_output, lax.axis_index("sp") * head_cols, head_cols, 1
    )

    def heads_first(matrix):
        return jnp.transpose(matrix.reshape(seq_length, head_count, head_width), (1, 0, 2))

    def tokens_first(matrix):
        return jnp.transpose(matrix, (1, 0, 2)).reshape(1, seq_length, head_cols)

    grads = head_grads(
        heads_first(query[0]),
        heads_first(keys[0]),
        heads_first(values[0]),
        heads_first(own_output),
        heads_first(head_cot[0]),
        cum[0],
    )
    query_grad, key_grad, value_grad = (
        lax.all_to_all(tokens_first(grads[0]), "sp", split_axis=1, concat_axis=2, tiled=True),
        lax.all_to_all(tokens_first(grads[1]), "sp", split_axis=1, concat_axis=2, tiled=True),
        lax.all_to_all(tokens_first(grads[2]), "sp", split_axis=1, concat_axis=2, tiled=True),
    )
    return (query_grad, key_grad, value_grad, grads[3][None], grad_weight)


def plain_solution(mesh):
    placed = (
        P("dp", None, "sp"),
        P("dp", None, "sp"),
        P("dp", None, "sp"),
        P("dp", None, None),
        P("dp", "sp", None),
        P("dp", "sp", None),
        P("dp", None),
    )
    return jax.shard_map(
        shards,
        mesh=mesh,
        in_specs=placed,
        out_specs=(
            P("dp", "sp", None),
            P("dp", "sp", None),
            P("dp", "sp", None),
            P("dp", "sp", None),
            P("dp", "sp"),
        ),
        check_vma=False,
    )


MESH = pl.DeviceIdType.MESH
PAIR = 2
LANES = 128


def nt(left, right):
    return lax.dot_general(
        left, right, (((1,), (1,)), ((), ())), preferred_element_type=jnp.float32
    )


def nn(left, right):
    return lax.dot_general(
        left, right, (((1,), (0,)), ((), ())), preferred_element_type=jnp.float32
    )


def kernel(
    n_sp, n_dp, n_heads, w_chunks,
    q_hbm, k_hbm, v_hbm, o_hbm, cum_hbm, do_hbm, w_hbm,
    dq_out, dk_out, dv_out, dcum_out, dw_out,
    q_ref, k_ref, v_ref, o_ref, cum_ref, dof, wbuf, prob, k_t, o_t,
    dw_own, y_send, y_recv, z_send, z_recv, dw_acc, stage, dcum_ref,
    in_sem, out_sem,
    x_ssem, x_rsem, c_ssem, c_rsem, f_ssem, f_rsem,
    wz_ssem, wz_rsem, wy_ssem, wy_rsem,
    ry_ssem, ry_rsem, rz_ssem, rz_rsem,
    g_ssem, g_rsem, g_lsem,
):
    sp, dp = lax.axis_index("sp"), lax.axis_index("dp")
    n_x, n_z = n_sp // PAIR, n_dp // PAIR
    x, core = sp // PAIR, sp % PAIR
    z, y = dp // PAIR, dp % PAIR
    length, head_cols = q_ref.shape
    head_width = head_cols // n_heads
    tokens, width = do_hbm.shape[1:]
    w_rows = w_hbm.shape[0]
    col_part = width // n_sp
    scale = head_width ** (-0.5)
    per_pair = LANES // head_width
    n_pairs = head_cols // LANES
    block = min(2 * LANES, length)
    n_blocks = length // block
    core_peer = x * PAIR + (1 - core)
    y_peer = z * PAIR + (1 - y)

    def token_rows(owner):
        return pl.ds(pl.multiple_of(owner * tokens, tokens), tokens)

    def col_at(part):
        return pl.ds(pl.multiple_of(part * col_part, LANES), col_part)

    def remote(src, dst, ssem, rsem, **where):
        return pltpu.make_async_remote_copy(
            src_ref=src, dst_ref=dst, send_sem=ssem, recv_sem=rsem,
            device_id=where, device_id_type=MESH,
        )

    own_w = pl.ds(pl.multiple_of(y * w_rows, w_rows), w_rows)
    loads = [
        pltpu.make_async_copy(do_hbm.at[0], dof.at[token_rows(sp)], in_sem.at[0]),
        pltpu.make_async_copy(q_hbm.at[0], q_ref, in_sem.at[2]),
        pltpu.make_async_copy(k_hbm.at[0], k_ref, in_sem.at[3]),
        pltpu.make_async_copy(cum_hbm.at[0], cum_ref, in_sem.at[4]),
        pltpu.make_async_copy(v_hbm.at[0], v_ref, in_sem.at[5]),
        pltpu.make_async_copy(o_hbm.at[0], o_ref, in_sem.at[6]),
    ]
    w_load = pltpu.make_async_copy(w_hbm, wbuf.at[own_w], in_sem.at[1])
    loads[0].start()

    @pl.when(z == sp)
    def _():
        w_load.start()

    for load in loads[1:]:
        load.start()

    barrier = pltpu.get_barrier_semaphore()
    for off in range(1, n_sp):
        pl.semaphore_signal(
            barrier, inc=1, device_id={"sp": (sp + off) % n_sp, "dp": dp}, device_id_type=MESH
        )
    for off in range(1, n_z):
        pl.semaphore_signal(
            barrier, inc=1,
            device_id={"sp": sp, "dp": ((z + off) % n_z) * PAIR + y}, device_id_type=MESH,
        )
    pl.semaphore_signal(barrier, inc=1, device_id={"sp": sp, "dp": y_peer}, device_id_type=MESH)
    pl.semaphore_wait(barrier, n_sp + n_z - 1)

    def x_copy(off, i, owner_x, target_x):
        part = dof.at[token_rows(owner_x * PAIR + core), col_at((target_x * PAIR + i) % n_sp)]
        return remote(part, part, x_ssem.at[off - 1, i], x_rsem.at[off - 1, i],
                      sp=target_x * PAIR + core, dp=dp)

    def x_out(off, i):
        return x_copy(off, i, x, (x + off) % n_x)

    def x_in(off, i):
        return x_copy(off, i, (x + n_x - off) % n_x, x)

    def core_copy(owner):
        part = dof.at[token_rows(owner)]
        return remote(part, part, c_ssem, c_rsem, sp=core_peer, dp=dp)

    def forward_copy(off, i, owner_core):
        owner = ((x + n_x - off) % n_x) * PAIR + owner_core
        part = dof.at[token_rows(owner), col_at((x * PAIR + i) % n_sp)]
        return remote(part, part, f_ssem.at[off - 1, i], f_rsem.at[off - 1, i],
                      sp=core_peer, dp=dp)

    loads[0].wait()
    for i in range(n_sp):
        for off in range(1, n_x):
            x_out(off, i).start()
    core_copy(sp).start()

    def forward_step(i):
        for off in range(1, n_x):
            x_in(off, i).wait_recv()
            forward_copy(off, i, core).start()

    chunk_rows = w_rows // w_chunks

    def w_part(owner_y, c):
        start = pl.multiple_of(owner_y * w_rows + c * chunk_rows, chunk_rows)
        return wbuf.at[pl.ds(start, chunk_rows)]

    def wz_copy(way, c, target_z):
        return remote(w_part(y, c), w_part(y, c), wz_ssem.at[way, c], wz_rsem.at[c],
                      sp=sp, dp=target_z * PAIR + y)

    def wy_copy(owner_y, c):
        return remote(w_part(owner_y, c), w_part(owner_y, c), wy_ssem.at[c], wy_rsem.at[c],
                      sp=sp, dp=y_peer)

    sends_up = jnp.logical_and(z >= sp, z < n_z - 1)
    sends_down = jnp.logical_and(z <= sp, z > 0)

    def w_send(c):
        @pl.when(sends_up)
        def _():
            wz_copy(0, c, z + 1).start()

        @pl.when(sends_down)
        def _():
            wz_copy(1, c, z - 1).start()

        wy_copy(y, c).start()

    @pl.when(z == sp)
    def _():
        w_load.wait()
        for c in range(w_chunks):
            w_send(c)

    def w_step(c):
        @pl.when(z != sp)
        def _():
            wz_copy(0, c, z).wait_recv()
            w_send(c)

    lane = lax.broadcasted_iota(jnp.int32, (1, LANES), 1)

    def head_mask(sub):
        return lane // head_width == sub

    def pair_cols(pair):
        return pl.ds(pl.multiple_of(pair * LANES, LANES), LANES)

    for load in loads[1:4]:
        load.wait()
    cum = cum_ref[...]
    cum_cols = jnp.concatenate([cum] * (-(-8 // n_heads)), axis=0).T

    def masked_query(pair, sub):
        return jnp.where(head_mask(sub), q_ref[:, pair_cols(pair)], 0)

    def probabilities(h):
        keys = k_ref[:, pair_cols(h // per_pair)]
        query = masked_query(h // per_pair, h % per_pair)
        for b in range(n_blocks):
            lo, end = b * block, (b + 1) * block
            scores = nt(keys[:end], query[lo:end]) * scale
            scores = scores + cum[h:h + 1, lo:end] - cum_cols[:end, h:h + 1]
            key_pos = lax.broadcasted_iota(jnp.int32, (end, block), 0)
            query_pos = lo + lax.broadcasted_iota(jnp.int32, (end, block), 1)
            scores = jnp.where(key_pos <= query_pos, scores, -1e30)
            weights = jnp.exp(scores - jnp.max(scores, axis=0, keepdims=True))
            weights = weights * (1.0 / jnp.sum(weights, axis=0, keepdims=True))
            prob[h, :end, lo:end] = weights

    def key_transpose():
        k_t[...] = k_ref[...].T

    def output_transpose():
        loads[4].wait()
        loads[5].wait()
        o_t[...] = o_ref[...].T

    def z_at(k):
        bits = [(b, (z // b) % 2) for b in (2**i for i in range(n_z.bit_length() - 1))]
        return sum(b * (1 - bit if k & b else bit) for b, bit in bits)

    def dw_rows(k, owner_y):
        return pl.ds(pl.multiple_of((z_at(k) * PAIR + owner_y) * w_rows, w_rows), w_rows)

    def ry_copy(k):
        return remote(y_send.at[k], y_recv.at[k], ry_ssem.at[k], ry_rsem.at[k], sp=sp, dp=y_peer)

    def rz_copy(k):
        return remote(z_send.at[k], z_recv.at[k], rz_ssem.at[k], rz_rsem.at[k],
                      sp=sp, dp=z_at(k) * PAIR + y)

    half = n_z // 2
    z_order = list(range(half, n_z)) + list(range(half - 1, -1, -1))
    def columns_arrive(first, last):
        for i in range(first, last):
            for off in range(1, n_x):
                forward_copy(off, i, 1 - core).wait_recv()

    def columns_ready():
        core_copy(core_peer).wait_recv()
        columns_arrive(0, PAIR)

    def dw_away(n):
        k = z_order[n]
        product = nn(o_t[dw_rows(k, 1 - y), :], dof[:, col_at(sp)])
        y_send[k] = product.astype(jnp.bfloat16)

    def dw_keep(n):
        k = z_order[n]
        dw_own[k] = nn(o_t[dw_rows(k, y), :], dof[:, col_at(sp)])

    def dw_exchange(n):
        ry_copy(z_order[n]).start()

    def dw_step(n):
        k = z_order[n]
        ry_copy(k).wait_recv()
        total = dw_own[k] + y_recv[k].astype(jnp.float32)
        if k == 0:
            dw_acc[...] = total
        else:
            z_send[k] = total.astype(jnp.bfloat16)
            rz_copy(k).start()

    outs = (dq_out, dk_out, dv_out)

    def grad_cols(pair):
        return pl.ds(pl.multiple_of(sp * head_cols + pair * LANES, LANES), LANES)

    def pair_of(turn):
        return y if turn == 0 else 1 - y

    def grad_copy(a, turn, off):
        target = (sp + off) % n_sp
        pair = pair_of(turn)
        return remote(stage.at[a, token_rows(target), pair_cols(pair)],
                      outs[a].at[0, :, grad_cols(pair)],
                      g_ssem.at[a, turn, off - 1], g_rsem.at[a, turn, off - 1], sp=target, dp=dp)

    def grad_keep(a, turn):
        pair = pair_of(turn)
        return pltpu.make_async_copy(stage.at[a, token_rows(sp), pair_cols(pair)],
                                     outs[a].at[0, :, grad_cols(pair)], g_lsem.at[a, turn])

    def add_rows(totals, part):
        for b in range(part.shape[0] // block):
            piece = part[b * block:(b + 1) * block]
            totals[b] = piece if totals[b] is None else totals[b] + piece

    def pair_gradients(turn):
        pair = pair_of(turn)
        if turn:
            for c in range(w_chunks):
                wy_copy(1 - y, c).wait_recv()
        pair_w = wbuf[pl.ds(pl.multiple_of(pair * w_rows, w_rows), w_rows), :]
        cot = nt(dof[...], pair_w).astype(jnp.bfloat16)
        own_out = o_ref[:, grad_cols(pair)]
        values = v_ref[:, pair_cols(pair)]
        row = lax.broadcasted_iota(jnp.int32, (8, LANES), 0)
        picks = (lax.broadcasted_iota(jnp.int32, (8, LANES), 1) // head_width == row)
        dots = lax.dot_general(
            picks.astype(jnp.float32), cot.astype(jnp.float32) * own_out.astype(jnp.float32),
            (((1,), (1,)), ((), ())), precision=lax.Precision.HIGHEST,
            preferred_element_type=jnp.float32,
        )
        key_total, value_total, query_total = [None] * n_blocks, [None] * n_blocks, []
        for sub in range(per_pair):
            h = pair * per_pair + sub
            cot_h = jnp.where(head_mask(sub), cot, 0)
            query_h = masked_query(pair, sub)
            keys_t = k_t[pl.ds(pl.multiple_of(h * head_width, head_width), head_width), :]
            query_parts, row_sums, col_sums = [], [], [None] * n_blocks
            for b in range(n_blocks):
                lo, end = b * block, (b + 1) * block
                weights = prob[h, :end, lo:end]
                d_prob = nt(values[:end], cot_h[lo:end])
                score_b = (weights * (d_prob - dots[sub:sub + 1, lo:end])).astype(jnp.bfloat16)
                add_rows(value_total, nn(weights.astype(jnp.bfloat16), cot_h[lo:end]))
                add_rows(key_total, nn(score_b, query_h[lo:end]))
                query_parts.append(nn(keys_t[:, :end], score_b))
                row_sums.append(nn(jnp.ones((8, end), jnp.bfloat16), score_b))
                col_sum = nt(jnp.ones((8, block), jnp.bfloat16), score_b)
                for j in range(b + 1):
                    piece = col_sum[:, j * block:(j + 1) * block]
                    col_sums[j] = piece if col_sums[j] is None else col_sums[j] + piece
            d_cum = jnp.concatenate(row_sums, axis=1) - jnp.concatenate(col_sums, axis=1)
            dcum_ref[pl.ds(h, 1), :] = d_cum[:1]
            query_total.append(jnp.concatenate(query_parts, axis=1))
        cols = pair_cols(pair)
        stage[0, :, cols] = (jnp.concatenate(query_total, axis=0).T * scale).astype(jnp.bfloat16)
        stage[1, :, cols] = (jnp.concatenate(key_total, axis=0) * scale).astype(jnp.bfloat16)
        stage[2, :, cols] = jnp.concatenate(value_total, axis=0).astype(jnp.bfloat16)
        for off in range(1, n_sp):
            for a in range(3):
                grad_copy(a, turn, off).start()
        for a in range(3):
            grad_keep(a, turn).start()

    output_transpose()
    key_transpose()
    for h in range(n_heads):
        probabilities(h)
    sent = 0
    for i in range(n_sp):
        upto = min(w_chunks * (i + 1) // n_sp + 1, w_chunks)
        for c in range(sent, upto):
            w_step(c)
        sent = upto
        forward_step(i)
    columns_ready()
    for n in range(half):
        dw_away(n)
        dw_exchange(n)
    columns_arrive(PAIR, n_sp)
    pair_gradients(0)
    for n in range(half, n_z):
        dw_away(n)
        dw_exchange(n)
    for n in range(n_z):
        dw_keep(n)
    dw_step(0)
    pair_gradients(1)
    for n in range(1, n_z):
        dw_step(n)

    total = dw_acc[...]
    for k in range(1, n_z):
        rz_copy(k).wait_recv()
        total = total + z_recv[k].astype(jnp.float32)
    dw_acc[...] = total
    results = [
        pltpu.make_async_copy(dw_acc, dw_out, out_sem.at[0]),
        pltpu.make_async_copy(dcum_ref, dcum_out.at[0], out_sem.at[1]),
    ]
    for result in results:
        result.start()

    for i in range(n_sp):
        for off in range(1, n_x):
            x_out(off, i).wait_send()
            forward_copy(off, i, core).wait_send()
    core_copy(sp).wait_send()
    for c in range(w_chunks):
        wy_copy(y, c).wait_send()

        @pl.when(sends_up)
        def _():
            wz_copy(0, c, z + 1).wait_send()

        @pl.when(sends_down)
        def _():
            wz_copy(1, c, z - 1).wait_send()

    for k in range(n_z):
        ry_copy(k).wait_send()
        if k:
            rz_copy(k).wait_send()
    for turn in range(n_pairs):
        for a in range(3):
            for off in range(1, n_sp):
                grad_copy(a, turn, off).wait()
            grad_keep(a, turn).wait()
    for result in results:
        result.wait()


def hand_over(*refs):
    count = len(refs) // 2
    copies = [
        pltpu.make_async_copy(refs[i], refs[count + i], refs[-1].at[i]) for i in range(count)
    ]
    for copy in copies:
        copy.start()
    for copy in copies:
        copy.wait()


def fits(mesh, query, cum, d_out, w_out):
    n_sp, n_dp = mesh.shape["sp"], mesh.shape["dp"]
    head_cols, n_heads = query.shape[2] // n_sp, cum.shape[1] // n_sp
    length, width = d_out.shape[1], d_out.shape[2]
    w_rows = w_out.shape[0] // n_dp
    if head_cols % LANES or n_heads == 0 or 8 % n_heads:
        return False
    if LANES % (head_cols // n_heads) or length % (2 * LANES) or (width // n_sp) % LANES:
        return False
    if n_sp & (n_sp - 1) or n_sp < PAIR or n_dp != PAIR * n_sp or head_cols != PAIR * LANES or w_rows != LANES:
        return False
    held = 4 * n_heads * length**2 + 2 * length * width + 8 * length * query.shape[2]
    return held < 32 * 2**20


def fused_shards(n_sp, n_dp, query, keys, values, output, cum, d_out, w_out):
    arrays = (query, keys, values, output, cum, d_out, w_out)
    length, head_cols = query.shape[1:]
    attn = output.shape[2]
    n_heads = cum.shape[1]
    tokens, width = d_out.shape[1:]
    w_rows = w_out.shape[0]
    n_x, n_z, col_part = n_sp // PAIR, n_dp // PAIR, width // n_sp
    w_chunks = 8
    bf16, f32 = jnp.bfloat16, jnp.float32
    dma = pltpu.SemaphoreType.DMA
    n_pairs = head_cols // LANES
    anywhere = pl.BlockSpec(memory_space=pl.ANY)
    from_hbm = pl.BlockSpec(memory_space=pltpu.HBM)
    grad = jax.ShapeDtypeStruct((1, tokens, attn), bf16)
    found = pl.pallas_call(
        functools.partial(kernel, n_sp, n_dp, n_heads, w_chunks),
        out_shape=(
            grad, grad, grad,
            jax.ShapeDtypeStruct(cum.shape, f32),
            jax.ShapeDtypeStruct((w_rows, col_part), f32),
        ),
        in_specs=[from_hbm] * 7,
        out_specs=[anywhere] * 5,
        scratch_shapes=[
            pltpu.VMEM((length, head_cols), bf16),
            pltpu.VMEM((length, head_cols), bf16),
            pltpu.VMEM((length, head_cols), bf16),
            pltpu.VMEM((length, attn), bf16),
            pltpu.VMEM(cum.shape[1:], f32),
            pltpu.VMEM((length, width), bf16),
            pltpu.VMEM((PAIR * w_rows, width), bf16),
            pltpu.VMEM((n_heads, length, length), f32),
            pltpu.VMEM((head_cols, length), bf16),
            pltpu.VMEM((attn, length), bf16),
            pltpu.VMEM((n_z, w_rows, col_part), f32),
            pltpu.VMEM((n_z, w_rows, col_part), bf16),
            pltpu.VMEM((n_z, w_rows, col_part), bf16),
            pltpu.VMEM((n_z, w_rows, col_part), bf16),
            pltpu.VMEM((n_z, w_rows, col_part), bf16),
            pltpu.VMEM((w_rows, col_part), f32),
            pltpu.VMEM((3, length, head_cols), bf16),
            pltpu.VMEM(cum.shape[1:], f32),
            dma((7,)), dma((2,)),
            dma((n_x - 1, n_sp)), dma((n_x - 1, n_sp)), dma, dma,
            dma((n_x - 1, n_sp)), dma((n_x - 1, n_sp)),
            dma((2, w_chunks)), dma((w_chunks,)), dma((w_chunks,)), dma((w_chunks,)),
            dma((n_z,)), dma((n_z,)), dma((n_z,)), dma((n_z,)),
            dma((3, n_pairs, n_sp - 1)), dma((3, n_pairs, n_sp - 1)), dma((3, n_pairs)),
        ],
        compiler_params=pltpu.CompilerParams(
            collective_id=0, has_side_effects=True, vmem_limit_bytes=48 * 2**20
        ),
    )(*[pltpu.with_memory_space_constraint(array, pltpu.HBM) for array in arrays])
    return pl.pallas_call(
        hand_over,
        out_shape=[jax.ShapeDtypeStruct(part.shape, part.dtype) for part in found],
        in_specs=[anywhere] * len(found),
        out_specs=[from_hbm] * len(found),
        scratch_shapes=[dma((len(found),))],
        compiler_params=pltpu.CompilerParams(vmem_limit_bytes=2**20),
    )(*found)


def solution(mesh):
    n_sp, n_dp = mesh.shape["sp"], mesh.shape["dp"]
    placed = (
        P("dp", None, "sp"), P("dp", None, "sp"), P("dp", None, "sp"), P("dp", None, None),
        P("dp", "sp", None), P("dp", "sp", None), P("dp", None),
    )
    results = (
        P("dp", "sp", None), P("dp", "sp", None), P("dp", "sp", None), P("dp", "sp", None),
        P("dp", "sp"),
    )

    def run(query, keys, values, output, cum, d_out, w_out):
        if fits(mesh, query, cum, d_out, w_out):
            body = functools.partial(fused_shards, n_sp, n_dp)
            step = jax.shard_map(
                body, mesh=mesh, in_specs=placed, out_specs=results, check_vma=False
            )
        else:
            step = plain_solution(mesh)
        return step(query, keys, values, output, cum, d_out, w_out)

    return run
```

profile of v0, /device:TPU:0, one launch (start us, length us, event | category | flops | bytes accessed | tf_op | source)
XLA Modules:
  0.0 41.7 jit_solution(5641374211054466230)
XLA Ops:
  0.6 40.0 %shard_map.110 = (bf16[1,128,1024]{2,1,0:T(8,128)(2,1)S(1)}, bf16[1,128,1024]{2,1,0:T(8,128)(2,1)S(1)}, bf16[1,128,1024]{2,1,0:T(8,128)(2,1)S(1)}, f32[1,4,512]{2,1,0:T(4,128)S(1)}, f32[128,512]{1,0:T(8,128)S(1)}) custom-call(bf16[1,512,256]{2,1,0:T(8,128)(2,1)} %q_hbm.1, bf16[1,512,256]{2,1,0:T(8,128)(2,1)} %k_hbm.1, bf16[1,512,256]{2,1,0:T(8,128)(2,1)} %v_hbm.1, ...), custom_call_target="tpu_custom_call" | custom-call | tf_op jit(solution)/shard_map/pallas_call | solution.py:569
  40.7 1.0 %shard_map.111 = (bf16[1,128,1024]{2,1,0:T(8,128)(2,1)}, bf16[1,128,1024]{2,1,0:T(8,128)(2,1)}, bf16[1,128,1024]{2,1,0:T(8,128)(2,1)}, f32[1,4,512]{2,1,0:T(4,128)}, f32[128,512]{1,0:T(8,128)}) custom-call(bf16[1,128,1024]{2,1,0:T(8,128)(2,1)S(1)} %get-tuple-element.10.refs_0_, bf16[1,128,1024]{2,1,0:T(8,128)(2,1)S(1)} %get-tuple-element.11.refs_1_, ...), custom_call_target="tpu_custom_call" | custom-call | tf_op jit(solution)/shard_map/pallas_call | solution.py:608
where the time goes:
time: 41.8 us; the launch traced here: 41.7 us
  Pallas kernels  41 us (98%)
  between operations  0.64 us (2%)
    pallas_call x1, Pallas kernels, fused_shards(): pl.pallas_call(functools.partial(kernel, n_sp, n_dp, n_heads, w_chunks),...  40 us
    pallas_call x1, Pallas kernels, fused_shards(): pl.pallas_call(hand_over, out_shape=[jax.ShapeDtypeStruct(part.shape, par...  1.01 us

commit v1 on v0

--- a/solution.py
+++ b/solution.py
@@ -1,3 +1,4 @@
+import contextlib
 import functools
 
 import jax
@@ -137,6 +138,7 @@
 
 
 MESH = pl.DeviceIdType.MESH
+ns = contextlib.nullcontext
 PAIR = 2
 LANES = 128
 
@@ -157,8 +159,8 @@
     n_sp, n_dp, n_heads, w_chunks,
     q_hbm, k_hbm, v_hbm, o_hbm, cum_hbm, do_hbm, w_hbm,
     dq_out, dk_out, dv_out, dcum_out, dw_out,
-    q_ref, k_ref, v_ref, o_ref, cum_ref, dof, wbuf, prob, k_t, o_t,
-    dw_own, y_send, y_recv, z_send, z_recv, dw_acc, stage, dcum_ref,
+    q_ref, k_ref, v_ref, o_ref, cum_ref, dof, wbuf, prob, prob_b, k_t, o_t,
+    dw_part, y_send, y_recv, z_send, z_recv, dw_acc, stage, dcum_ref,
     in_sem, out_sem,
     x_ssem, x_rsem, c_ssem, c_rsem, f_ssem, f_rsem,
     wz_ssem, wz_rsem, wy_ssem, wy_rsem,
@@ -166,7 +168,7 @@
     g_ssem, g_rsem, g_lsem,
 ):
     sp, dp = lax.axis_index("sp"), lax.axis_index("dp")
-    n_x, n_z = n_sp // PAIR, n_dp // PAIR
+    n_z = n_dp // PAIR
     x, core = sp // PAIR, sp % PAIR
     z, y = dp // PAIR, dp % PAIR
     length, head_cols = q_ref.shape
@@ -226,37 +228,40 @@
     pl.semaphore_signal(barrier, inc=1, device_id={"sp": sp, "dp": y_peer}, device_id_type=MESH)
     pl.semaphore_wait(barrier, n_sp + n_z - 1)
 
-    def x_copy(off, i, owner_x, target_x):
-        part = dof.at[token_rows(owner_x * PAIR + core), col_at((target_x * PAIR + i) % n_sp)]
-        return remote(part, part, x_ssem.at[off - 1, i], x_rsem.at[off - 1, i],
-                      sp=target_x * PAIR + core, dp=dp)
-
-    def x_out(off, i):
-        return x_copy(off, i, x, (x + off) % n_x)
-
-    def x_in(off, i):
-        return x_copy(off, i, (x + n_x - off) % n_x, x)
+    def chip_rows(owner_x):
+        return pl.ds(pl.multiple_of(owner_x * PAIR * tokens, PAIR * tokens), PAIR * tokens)
+
+    def x_out(i):
+        part = dof.at[token_rows(sp), col_at(((1 - x) * PAIR + i) % n_sp)]
+        slot, target_core = (0, i) if i < PAIR else (i - 1, core)
+        return remote(part, part, x_ssem, x_rsem.at[slot], sp=(1 - x) * PAIR + target_core, dp=dp)
+
+    def arrived(i, owner_core):
+        if i == 0:
+            return dof.at[chip_rows(1 - x), col_at(x * PAIR + owner_core)]
+        owner = (1 - x) * PAIR + owner_core
+        return dof.at[token_rows(owner), col_at((x * PAIR + i + 1) % n_sp)]
+
+    def x_in(i):
+        part = arrived(i, core)
+        return remote(part, part, x_ssem, x_rsem.at[i], sp=core_peer, dp=dp)
 
     def core_copy(owner):
         part = dof.at[token_rows(owner)]
         return remote(part, part, c_ssem, c_rsem, sp=core_peer, dp=dp)
 
-    def forward_copy(off, i, owner_core):
-        owner = ((x + n_x - off) % n_x) * PAIR + owner_core
-        part = dof.at[token_rows(owner), col_at((x * PAIR + i) % n_sp)]
-        return remote(part, part, f_ssem.at[off - 1, i], f_rsem.at[off - 1, i],
-                      sp=core_peer, dp=dp)
-
-    loads[0].wait()
-    for i in range(n_sp):
-        for off in range(1, n_x):
-            x_out(off, i).start()
-    core_copy(sp).start()
+    def forward_copy(i, owner_core):
+        part = arrived(i, owner_core)
+        return remote(part, part, f_ssem, f_rsem.at[min(i, 1)], sp=core_peer, dp=dp)
+
+    def x_start():
+        loads[0].wait()
+        for i in range(n_sp):
+            x_out(i).start()
 
     def forward_step(i):
-        for off in range(1, n_x):
-            x_in(off, i).wait_recv()
-            forward_copy(off, i, core).start()
+        x_in(i).wait_recv()
+        forward_copy(i, core).start()
 
     chunk_rows = w_rows // w_chunks
 
@@ -265,11 +270,11 @@
         return wbuf.at[pl.ds(start, chunk_rows)]
 
     def wz_copy(way, c, target_z):
-        return remote(w_part(y, c), w_part(y, c), wz_ssem.at[way, c], wz_rsem.at[c],
+        return remote(w_part(y, c), w_part(y, c), wz_ssem.at[way], wz_rsem.at[c],
                       sp=sp, dp=target_z * PAIR + y)
 
     def wy_copy(owner_y, c):
-        return remote(w_part(owner_y, c), w_part(owner_y, c), wy_ssem.at[c], wy_rsem.at[c],
+        return remote(w_part(owner_y, c), w_part(owner_y, c), wy_ssem, wy_rsem,
                       sp=sp, dp=y_peer)
 
     sends_up = jnp.logical_and(z >= sp, z < n_z - 1)
@@ -284,19 +289,33 @@
         def _():
             wz_copy(1, c, z - 1).start()
 
+    def w_cross(c):
         wy_copy(y, c).start()
+
+    near = z // PAIR == x
+    far = z // PAIR != x
+    held = w_chunks - 2
 
     @pl.when(z == sp)
     def _():
         w_load.wait()
         for c in range(w_chunks):
             w_send(c)
-
-    def w_step(c):
+        x_start()
+        for c in range(held):
+            w_cross(c)
+
+    @pl.when(z != sp)
+    def _():
+        x_start()
+
+    def w_step(c, cross=True):
         @pl.when(z != sp)
         def _():
             wz_copy(0, c, z).wait_recv()
             w_send(c)
+            if cross:
+                w_cross(c)
 
     lane = lax.broadcasted_iota(jnp.int32, (1, LANES), 1)
 
@@ -327,6 +346,7 @@
             weights = jnp.exp(scores - jnp.max(scores, axis=0, keepdims=True))
             weights = weights * (1.0 / jnp.sum(weights, axis=0, keepdims=True))
             prob[h, :end, lo:end] = weights
+            prob_b[h, :end, lo:end] = weights.astype(jnp.bfloat16)
 
     def key_transpose():
         k_t[...] = k_ref[...].T
@@ -336,52 +356,53 @@
         loads[5].wait()
         o_t[...] = o_ref[...].T
 
-    def z_at(k):
-        bits = [(b, (z // b) % 2) for b in (2**i for i in range(n_z.bit_length() - 1))]
-        return sum(b * (1 - bit if k & b else bit) for b, bit in bits)
-
-    def dw_rows(k, owner_y):
-        return pl.ds(pl.multiple_of((z_at(k) * PAIR + owner_y) * w_rows, w_rows), w_rows)
-
-    def ry_copy(k):
-        return remote(y_send.at[k], y_recv.at[k], ry_ssem.at[k], ry_rsem.at[k], sp=sp, dp=y_peer)
-
-    def rz_copy(k):
-        return remote(z_send.at[k], z_recv.at[k], rz_ssem.at[k], rz_rsem.at[k],
-                      sp=sp, dp=z_at(k) * PAIR + y)
-
-    half = n_z // 2
-    z_order = list(range(half, n_z)) + list(range(half - 1, -1, -1))
-    def columns_arrive(first, last):
-        for i in range(first, last):
-            for off in range(1, n_x):
-                forward_copy(off, i, 1 - core).wait_recv()
-
-    def columns_ready():
-        core_copy(core_peer).wait_recv()
-        columns_arrive(0, PAIR)
-
-    def dw_away(n):
-        k = z_order[n]
-        product = nn(o_t[dw_rows(k, 1 - y), :], dof[:, col_at(sp)])
-        y_send[k] = product.astype(jnp.bfloat16)
-
-    def dw_keep(n):
-        k = z_order[n]
-        dw_own[k] = nn(o_t[dw_rows(k, y), :], dof[:, col_at(sp)])
-
-    def dw_exchange(n):
-        ry_copy(z_order[n]).start()
-
-    def dw_step(n):
-        k = z_order[n]
-        ry_copy(k).wait_recv()
-        total = dw_own[k] + y_recv[k].astype(jnp.float32)
-        if k == 0:
-            dw_acc[...] = total
-        else:
-            z_send[k] = total.astype(jnp.bfloat16)
-            rz_copy(k).start()
+    step_of = jnp.where(x == 0, z, n_z - 1 - z)
+
+    def dp_at(step, lane_y):
+        return jnp.where(x == 0, step, n_z - 1 - step) * PAIR + lane_y
+
+    def lane_of(other):
+        return 1 - y if other else y
+
+    def product(step, other):
+        row = pl.multiple_of(dp_at(step, lane_of(other)) * w_rows, w_rows)
+        return nn(o_t[pl.ds(row, w_rows), :], dof[:, col_at(sp)])
+
+    def keep(step, other):
+        dw_part[2 * step + other] = product(step, other)
+
+    def y_copy(slot):
+        return remote(y_send.at[slot], y_recv.at[slot], ry_ssem, ry_rsem.at[slot],
+                      sp=sp, dp=y_peer)
+
+    def z_copy(source, target, step):
+        return remote(z_send.at[source], z_recv.at[target], rz_ssem, rz_rsem.at[target],
+                      sp=sp, dp=dp_at(step, y))
+
+    def to_y(slot, value):
+        y_send[slot] = value.astype(jnp.bfloat16)
+        y_copy(slot).start()
+
+    def to_z(source, value, target, step):
+        z_send[source] = value.astype(jnp.bfloat16)
+        z_copy(source, target, step).start()
+
+    def from_y(slot):
+        y_copy(slot).wait_recv()
+        return y_recv[slot].astype(jnp.float32)
+
+    def from_z(target):
+        z_copy(0, target, step_of).wait_recv()
+        return z_recv[target].astype(jnp.float32)
+
+    def part_of(step, other):
+        return dw_part[2 * step + other]
+
+    def columns_arrive():
+        forward_copy(0, 1 - core).wait_recv()
+        first = pl.multiple_of((1 - x) * PAIR * col_part, PAIR * col_part)
+        part = dof.at[token_rows((1 - x) * PAIR + 1 - core), pl.ds(first, PAIR * col_part)]
+        remote(part, part, f_ssem, f_rsem.at[1], sp=core_peer, dp=dp).wait_recv()
 
     outs = (dq_out, dk_out, dv_out)
 
@@ -396,99 +417,326 @@
         pair = pair_of(turn)
         return remote(stage.at[a, token_rows(target), pair_cols(pair)],
                       outs[a].at[0, :, grad_cols(pair)],
-                      g_ssem.at[a, turn, off - 1], g_rsem.at[a, turn, off - 1], sp=target, dp=dp)
+                      g_ssem, g_rsem, sp=target, dp=dp)
 
     def grad_keep(a, turn):
         pair = pair_of(turn)
         return pltpu.make_async_copy(stage.at[a, token_rows(sp), pair_cols(pair)],
-                                     outs[a].at[0, :, grad_cols(pair)], g_lsem.at[a, turn])
+                                     outs[a].at[0, :, grad_cols(pair)], g_lsem)
 
     def add_rows(totals, part):
         for b in range(part.shape[0] // block):
             piece = part[b * block:(b + 1) * block]
             totals[b] = piece if totals[b] is None else totals[b] + piece
 
-    def pair_gradients(turn):
+    def send_grad(a, turn):
+        for off in range(1, n_sp):
+            grad_copy(a, turn, off).start()
+        grad_keep(a, turn).start()
+
+    def picked(left, pick):
+        high = left.astype(jnp.bfloat16)
+        low = (left - high.astype(jnp.float32)).astype(jnp.bfloat16)
+        row = lax.broadcasted_iota(jnp.int32, (8, 2 * LANES), 0)
+        column = lax.broadcasted_iota(jnp.int32, (8, 2 * LANES), 1) % LANES
+        picks = jnp.where(pick(row, column), 1.0, 0.0).astype(jnp.bfloat16)
+        return nt(picks, jnp.concatenate([high, low], axis=1))
+
+    def pair_gradients(turn, early, between):
         pair = pair_of(turn)
+        cols = pair_cols(pair)
         if turn:
-            for c in range(w_chunks):
-                wy_copy(1 - y, c).wait_recv()
-        pair_w = wbuf[pl.ds(pl.multiple_of(pair * w_rows, w_rows), w_rows), :]
-        cot = nt(dof[...], pair_w).astype(jnp.bfloat16)
-        own_out = o_ref[:, grad_cols(pair)]
-        values = v_ref[:, pair_cols(pair)]
-        row = lax.broadcasted_iota(jnp.int32, (8, LANES), 0)
-        picks = (lax.broadcasted_iota(jnp.int32, (8, LANES), 1) // head_width == row)
-        dots = lax.dot_general(
-            picks.astype(jnp.float32), cot.astype(jnp.float32) * own_out.astype(jnp.float32),
-            (((1,), (1,)), ((), ())), precision=lax.Precision.HIGHEST,
-            preferred_element_type=jnp.float32,
-        )
-        key_total, value_total, query_total = [None] * n_blocks, [None] * n_blocks, []
+            block_w = wbuf.at[pl.ds(pl.multiple_of((1 - y) * w_rows, w_rows), w_rows)]
+            remote(block_w, block_w, wy_ssem, wy_rsem, sp=sp, dp=y_peer).wait_recv()
+        with ns(f"pair{turn}a0"):
+            pair_w = wbuf[pl.ds(pl.multiple_of(pair * w_rows, w_rows), w_rows), :]
+            cot = nt(dof[...], pair_w).astype(jnp.bfloat16)
+            cots = [jnp.where(head_mask(sub), cot, 0) for sub in range(per_pair)]
+        with ns(f"pair{turn}a1"):
+            value_total = [None] * n_blocks
+            for sub in range(per_pair):
+                h = pair * per_pair + sub
+                for b in range(n_blocks):
+                    lo, end = b * block, (b + 1) * block
+                    add_rows(value_total, nn(prob_b[h, :end, lo:end], cots[sub][lo:end]))
+            stage[2, :, cols] = jnp.concatenate(value_total, axis=0).astype(jnp.bfloat16)
+            send_grad(2, turn)
+        early()
+        with ns(f"pair{turn}a2"):
+            own_out = o_ref[:, grad_cols(pair)]
+            values = v_ref[:, cols]
+            dots = picked(cot.astype(jnp.float32) * own_out.astype(jnp.float32),
+                          lambda row, column: column // head_width == row)
+        key_totals, query_total, row_sums = [], [], []
         for sub in range(per_pair):
-            h = pair * per_pair + sub
-            cot_h = jnp.where(head_mask(sub), cot, 0)
-            query_h = masked_query(pair, sub)
-            keys_t = k_t[pl.ds(pl.multiple_of(h * head_width, head_width), head_width), :]
-            query_parts, row_sums, col_sums = [], [], [None] * n_blocks
-            for b in range(n_blocks):
-                lo, end = b * block, (b + 1) * block
-                weights = prob[h, :end, lo:end]
-                d_prob = nt(values[:end], cot_h[lo:end])
-                score_b = (weights * (d_prob - dots[sub:sub + 1, lo:end])).astype(jnp.bfloat16)
-                add_rows(value_total, nn(weights.astype(jnp.bfloat16), cot_h[lo:end]))
-                add_rows(key_total, nn(score_b, query_h[lo:end]))
-                query_parts.append(nn(keys_t[:, :end], score_b))
-                row_sums.append(nn(jnp.ones((8, end), jnp.bfloat16), score_b))
-                col_sum = nt(jnp.ones((8, block), jnp.bfloat16), score_b)
-                for j in range(b + 1):
-                    piece = col_sum[:, j * block:(j + 1) * block]
-                    col_sums[j] = piece if col_sums[j] is None else col_sums[j] + piece
-            d_cum = jnp.concatenate(row_sums, axis=1) - jnp.concatenate(col_sums, axis=1)
-            dcum_ref[pl.ds(h, 1), :] = d_cum[:1]
-            query_total.append(jnp.concatenate(query_parts, axis=1))
-        cols = pair_cols(pair)
-        stage[0, :, cols] = (jnp.concatenate(query_total, axis=0).T * scale).astype(jnp.bfloat16)
-        stage[1, :, cols] = (jnp.concatenate(key_total, axis=0) * scale).astype(jnp.bfloat16)
-        stage[2, :, cols] = jnp.concatenate(value_total, axis=0).astype(jnp.bfloat16)
-        for off in range(1, n_sp):
-            for a in range(3):
-                grad_copy(a, turn, off).start()
-        for a in range(3):
-            grad_keep(a, turn).start()
-
-    output_transpose()
-    key_transpose()
-    for h in range(n_heads):
-        probabilities(h)
-    sent = 0
-    for i in range(n_sp):
-        upto = min(w_chunks * (i + 1) // n_sp + 1, w_chunks)
-        for c in range(sent, upto):
+            with ns(f"pair{turn}b{sub}"):
+                h = pair * per_pair + sub
+                spare = jnp.where(lane == (1 - sub) * head_width, 1.0, 0.0).astype(jnp.bfloat16)
+                query_h = jnp.where(head_mask(sub), q_ref[:, cols], spare)
+                keys_t = k_t[pl.ds(pl.multiple_of(h * head_width, head_width), head_width), :]
+                keys_t = jnp.concatenate([keys_t, jnp.ones((16, length), jnp.bfloat16)], axis=0)
+                key_total, query_parts = [None] * n_blocks, []
+                for b in range(n_blocks):
+                    lo, end = b * block, (b + 1) * block
+                    weights = prob[h, :end, lo:end]
+                    d_prob = nt(values[:end], cots[sub][lo:end])
+                    score_b = (weights * (d_prob - dots[sub:sub + 1, lo:end])).astype(jnp.bfloat16)
+                    add_rows(key_total, nn(score_b, query_h[lo:end]))
+                    query_parts.append(nn(keys_t[:, :end], score_b))
+                key_totals.append(jnp.concatenate(key_total, axis=0))
+                query_sums = jnp.concatenate(query_parts, axis=1)
+                query_total.append(query_sums[:head_width])
+                row_sums.append(query_sums[head_width:head_width + 1])
+            if sub == 0:
+                between()
+        with ns(f"pair{turn}c"):
+            first = head_mask(0)
+            key_grad = jnp.where(first, key_totals[0], key_totals[1])
+            stage[1, :, cols] = (key_grad * scale).astype(jnp.bfloat16)
+            send_grad(1, turn)
+            stage[0, :, cols] = (jnp.concatenate(query_total, axis=0).T * scale).astype(jnp.bfloat16)
+            send_grad(0, turn)
+            col_sums = picked(jnp.where(first, key_totals[1], key_totals[0]),
+                              lambda row, column: column == (1 - row) * head_width)
+            for sub in range(per_pair):
+                d_cum = row_sums[sub] - col_sums[sub:sub + 1]
+                dcum_ref[pl.ds(pair * per_pair + sub, 1), :] = d_cum
+
+    def at_step(step):
+        return lambda action: pl.when(step_of == step)(action)
+
+    with ns("a_prep"):
+        output_transpose()
+        key_transpose()
+        core_copy(sp).start()
+        for h in range(n_heads):
+            probabilities(h)
+
+    def relay(first, last):
+        for c in range(first, last):
             w_step(c)
-        sent = upto
-        forward_step(i)
-    columns_ready()
-    for n in range(half):
-        dw_away(n)
-        dw_exchange(n)
-    columns_arrive(PAIR, n_sp)
-    pair_gradients(0)
-    for n in range(half, n_z):
-        dw_away(n)
-        dw_exchange(n)
-    for n in range(n_z):
-        dw_keep(n)
-    dw_step(0)
-    pair_gradients(1)
-    for n in range(1, n_z):
-        dw_step(n)
-
-    total = dw_acc[...]
-    for k in range(1, n_z):
-        rz_copy(k).wait_recv()
-        total = total + z_recv[k].astype(jnp.float32)
-    dw_acc[...] = total
+
+    def columns_first(ahead):
+        lax.fori_loop(0, ahead, lambda c, done: (w_step(c), done)[1], 0)
+        forward_step(0)
+
+        core_copy(core_peer).wait_recv()
+
+    def w_later(c, ahead):
+        @pl.when(c >= ahead)
+        def _():
+            w_step(c)
+
+    def relay2(first, last):
+        for c in range(first, last):
+            w_later(c, ahead2)
+
+    def relay3(first, last):
+        for c in range(first, last):
+            w_later(c, ahead3)
+
+    def far_near(n):
+        step, other = n % 2, 1 - n // 2
+        value = product(step, other)
+
+        @at_step(3)
+        def _():
+            to_z(n, value, n, 2)
+
+        @at_step(2)
+        def _():
+            dw_part[2 * step + other] = value
+
+    def far_cross(slot, step):
+        y_send[slot] = product(step, 1).astype(jnp.bfloat16)
+
+    ahead2 = jnp.where(x == 0, core * w_chunks, 2)
+    ahead3 = jnp.where(x == 0, core * w_chunks, 0)
+
+    with ns("b_relay"):
+        @pl.when(near)
+        def _():
+            relay(0, 4)
+
+            @pl.when(core == 0)
+            def _():
+                forward_step(0)
+
+            for c in range(4, w_chunks):
+                w_step(c, c < held)
+
+            @pl.when(core == 1)
+            def _():
+                forward_step(0)
+
+            core_copy(core_peer).wait_recv()
+
+        @at_step(2)
+        def _():
+            columns_first(ahead2)
+
+        @at_step(3)
+        def _():
+            columns_first(ahead3)
+
+    with ns("d_dw"):
+        @pl.when(near)
+        def _():
+            sibling = 1 - step_of
+            to_y(0, product(3, 1))
+            to_y(1, product(2, 1))
+            for c in range(held, w_chunks):
+                w_cross(c)
+            to_z(0, product(sibling, 1), 2, sibling)
+            to_z(1, product(sibling, 0), 3, sibling)
+            keep(3, 0)
+            forward_step(1)
+            keep(2, 0)
+            keep(step_of, 1)
+            keep(step_of, 0)
+            forward_step(2)
+
+        @at_step(2)
+        def _():
+            relay2(0, 1)
+            far_near(0)
+            relay2(1, 2)
+            far_near(1)
+            relay2(2, 3)
+            far_near(2)
+            relay2(3, 4)
+            far_near(3)
+            relay2(4, 5)
+            far_cross(0, 3)
+            relay2(5, 6)
+            far_cross(1, 2)
+            relay2(6, 7)
+            keep(3, 0)
+            relay2(7, 8)
+            forward_step(1)
+            y_copy(0).start()
+            y_copy(1).start()
+            keep(2, 0)
+            forward_step(2)
+
+        @at_step(3)
+        def _():
+            for n in range(4):
+                far_near(n)
+
+            relay3(0, 2)
+            far_cross(0, 2)
+
+            @pl.when(x == 0)
+            def _():
+                forward_step(1)
+
+            relay3(2, 4)
+            far_cross(1, 3)
+
+            @pl.when(x == 0)
+            def _():
+                forward_step(2)
+
+            relay3(4, 6)
+            keep(2, 0)
+
+            @pl.when(x == 1)
+            def _():
+                forward_step(1)
+                forward_step(2)
+
+            keep(3, 0)
+            relay3(6, 8)
+            y_copy(0).start()
+            y_copy(1).start()
+
+    with ns("e_cols2"):
+        columns_arrive()
+
+    def pass_on(n):
+        step, other = n % 2, 1 - n // 2
+        to_z(n, part_of(step, other) + from_z(n), 1 - other, step)
+
+    def near_far(slot, step):
+        return part_of(step, 0) + from_y(slot)
+
+    def over_y():
+        to_y(2, part_of(step_of, 1) + from_z(0) + from_z(2))
+
+    with ns("f_poll"):
+        @at_step(0)
+        def _():
+            to_z(2, near_far(0, 3), 4, 1)
+
+        @at_step(1)
+        def _():
+            dw_part[6] = near_far(0, 3)
+
+        @at_step(2)
+        def _():
+            pass_on(0)
+
+    def between0():
+        with ns("g_poll"):
+            @at_step(0)
+            def _():
+                to_z(3, near_far(1, 2), 5, 2)
+
+            @at_step(1)
+            def _():
+                to_z(3, near_far(1, 2), 6, 2)
+
+            @at_step(2)
+            def _():
+                pass_on(1)
+
+    pair_gradients(0, lambda: None, between0)
+    with ns("h_poll"):
+        @at_step(2)
+        def _():
+            pass_on(2)
+            pass_on(3)
+
+    def early1():
+        with ns("i0_poll"):
+            @at_step(3)
+            def _():
+                to_z(4, part_of(2, 0) + from_y(0), 4, 2)
+
+    def between1():
+        with ns("i_poll"):
+            @at_step(0)
+            def _():
+                over_y()
+
+            @at_step(1)
+            def _():
+                to_z(2, part_of(3, 0) + from_z(4), 5, 3)
+
+            @at_step(2)
+            def _():
+                to_z(4, part_of(3, 0) + from_y(0), 4, 3)
+
+    pair_gradients(1, early1, between1)
+    with ns("j_poll"):
+        @at_step(1)
+        def _():
+            over_y()
+
+    with ns("k_final"):
+        @pl.when(near)
+        def _():
+            dw_acc[...] = part_of(step_of, 0) + from_z(1) + from_z(3) + from_y(2)
+
+        @at_step(2)
+        def _():
+            dw_acc[...] = part_of(2, 0) + from_y(1) + from_z(5) + from_z(6) + from_z(4)
+
+        @at_step(3)
+        def _():
+            dw_acc[...] = part_of(3, 0) + from_y(1) + from_z(4) + from_z(5)
+
     results = [
         pltpu.make_async_copy(dw_acc, dw_out, out_sem.at[0]),
         pltpu.make_async_copy(dcum_ref, dcum_out.at[0], out_sem.at[1]),
@@ -496,33 +744,44 @@
     for result in results:
         result.start()
 
-    for i in range(n_sp):
-        for off in range(1, n_x):
-            x_out(off, i).wait_send()
-            forward_copy(off, i, core).wait_send()
-    core_copy(sp).wait_send()
-    for c in range(w_chunks):
-        wy_copy(y, c).wait_send()
+    def sent(part, sem):
+        remote(part, part, sem, sem, sp=core_peer, dp=dp).wait_send()
+
+    own_rows = dof.at[token_rows(sp)]
+    block_w = wbuf.at[own_w]
+    rest = stage.at[:, pl.ds(0, length - tokens)]
+    with ns("o_waitsend"):
+        sent(own_rows, x_ssem)
+        sent(own_rows, f_ssem)
+        core_copy(sp).wait_send()
+        sent(block_w, wy_ssem)
 
         @pl.when(sends_up)
         def _():
-            wz_copy(0, c, z + 1).wait_send()
+            sent(block_w, wz_ssem.at[0])
 
         @pl.when(sends_down)
         def _():
-            wz_copy(1, c, z - 1).wait_send()
-
-    for k in range(n_z):
-        ry_copy(k).wait_send()
-        if k:
-            rz_copy(k).wait_send()
-    for turn in range(n_pairs):
-        for a in range(3):
-            for off in range(1, n_sp):
-                grad_copy(a, turn, off).wait()
-            grad_keep(a, turn).wait()
-    for result in results:
-        result.wait()
+            sent(block_w, wz_ssem.at[1])
+
+        @pl.when(near)
+        def _():
+            sent(y_send, ry_ssem)
+            sent(z_send.at[pl.ds(0, 4)], rz_ssem)
+
+        @pl.when(far)
+        def _():
+            sent(y_send.at[pl.ds(0, 2)], ry_ssem)
+            sent(z_send, rz_ssem)
+
+        sent(rest, g_ssem)
+    with ns("p_gradwait"):
+        remote(rest, rest, g_ssem, g_rsem, sp=core_peer, dp=dp).wait_recv()
+        kept = stage.at[:, pl.ds(0, tokens)]
+        pltpu.make_async_copy(kept, kept, g_lsem).wait()
+    with ns("q_results"):
+        for result in results:
+            result.wait()
 
 
 def hand_over(*refs):
@@ -543,11 +802,11 @@
     w_rows = w_out.shape[0] // n_dp
     if head_cols % LANES or n_heads == 0 or 8 % n_heads:
         return False
-    if LANES % (head_cols // n_heads) or length % (2 * LANES) or (width // n_sp) % LANES:
+    if LANES != PAIR * (head_cols // n_heads) or length % (2 * LANES) or (width // n_sp) % LANES:
         return False
-    if n_sp & (n_sp - 1) or n_sp < PAIR or n_dp != PAIR * n_sp or head_cols != PAIR * LANES or w_rows != LANES:
+    if n_sp & (n_sp - 1) or n_sp < PAIR or n_dp != PAIR * n_sp or n_sp != PAIR * PAIR or head_cols != PAIR * LANES or w_rows != LANES:
         return False
-    held = 4 * n_heads * length**2 + 2 * length * width + 8 * length * query.shape[2]
+    held = 6 * n_heads * length**2 + 2 * length * width + 8 * length * query.shape[2]
     return held < 32 * 2**20
 
 
@@ -558,7 +817,7 @@
     n_heads = cum.shape[1]
     tokens, width = d_out.shape[1:]
     w_rows = w_out.shape[0]
-    n_x, n_z, col_part = n_sp // PAIR, n_dp // PAIR, width // n_sp
+    n_z, col_part = n_dp // PAIR, width // n_sp
     w_chunks = 8
     bf16, f32 = jnp.bfloat16, jnp.float32
     dma = pltpu.SemaphoreType.DMA
@@ -584,22 +843,22 @@
             pltpu.VMEM((length, width), bf16),
             pltpu.VMEM((PAIR * w_rows, width), bf16),
             pltpu.VMEM((n_heads, length, length), f32),
+            pltpu.VMEM((n_heads, length, length), bf16),
             pltpu.VMEM((head_cols, length), bf16),
             pltpu.VMEM((attn, length), bf16),
-            pltpu.VMEM((n_z, w_rows, col_part), f32),
-            pltpu.VMEM((n_z, w_rows, col_part), bf16),
-            pltpu.VMEM((n_z, w_rows, col_part), bf16),
-            pltpu.VMEM((n_z, w_rows, col_part), bf16),
-            pltpu.VMEM((n_z, w_rows, col_part), bf16),
+            pltpu.VMEM((PAIR * n_z, w_rows, col_part), f32),
+            pltpu.VMEM((3, w_rows, col_part), bf16),
+            pltpu.VMEM((3, w_rows, col_part), bf16),
+            pltpu.VMEM((5, w_rows, col_part), bf16),
+            pltpu.VMEM((7, w_rows, col_part), bf16),
             pltpu.VMEM((w_rows, col_part), f32),
             pltpu.VMEM((3, length, head_cols), bf16),
             pltpu.VMEM(cum.shape[1:], f32),
             dma((7,)), dma((2,)),
-            dma((n_x - 1, n_sp)), dma((n_x - 1, n_sp)), dma, dma,
-            dma((n_x - 1, n_sp)), dma((n_x - 1, n_sp)),
-            dma((2, w_chunks)), dma((w_chunks,)), dma((w_chunks,)), dma((w_chunks,)),
-            dma((n_z,)), dma((n_z,)), dma((n_z,)), dma((n_z,)),
-            dma((3, n_pairs, n_sp - 1)), dma((3, n_pairs, n_sp - 1)), dma((3, n_pairs)),
+            dma, dma((n_sp - 1,)), dma, dma, dma, dma((PAIR,)),
+            dma((2,)), dma((w_chunks,)), dma, dma,
+            dma, dma((3,)), dma, dma((7,)),
+            dma, dma, dma,
         ],
         compiler_params=pltpu.CompilerParams(
             collective_id=0, has_side_effects=True, vmem_limit_bytes=48 * 2**20

time: 41.8 us -> 37.4 us (0.89)
  Pallas kernels: 41 us -> 36.6 us
    pallas_call x1, Pallas kernels: 40 us -> 35.6 us  [fused_shards(): pl.pallas_call(functools.partial(kernel, n_sp, n_dp, n_heads, w_chunks),...]
where the time goes in v1:
time: 37.4 us; the launch traced here: 37.2 us
  Pallas kernels  36.6 us (98%)
  between operations  0.64 us (2%)
    pallas_call x1, Pallas kernels, fused_shards(): pl.pallas_call(functools.partial(kernel, n_sp, n_dp, n_heads, w_chunks),...  35.6 us
    pallas_call x1, Pallas kernels, fused_shards(): pl.pallas_call(hand_over, out_shape=[jax.ShapeDtypeStruct(part.shape, par...  1.01 us

profile of v1, /device:TPU:0, one launch (start us, length us, event | category | flops | bytes accessed | tf_op | source)
XLA Modules:
  0.0 37.2 jit_solution(489270782269319690)
XLA Ops:
  0.6 35.6 %shard_map.110 = (bf16[1,128,1024]{2,1,0:T(8,128)(2,1)S(1)}, bf16[1,128,1024]{2,1,0:T(8,128)(2,1)S(1)}, bf16[1,128,1024]{2,1,0:T(8,128)(2,1)S(1)}, f32[1,4,512]{2,1,0:T(4,128)S(1)}, f32[128,512]{1,0:T(8,128)S(1)}) custom-call(bf16[1,512,256]{2,1,0:T(8,128)(2,1)} %q_hbm.1, bf16[1,512,256]{2,1,0:T(8,128)(2,1)} %k_hbm.1, bf16[1,512,256]{2,1,0:T(8,128)(2,1)} %v_hbm.1, ...), custom_call_target="tpu_custom_call" | custom-call | tf_op jit(solution)/shard_map/pallas_call | solution.py:828
  36.2 1.0 %shard_map.111 = (bf16[1,128,1024]{2,1,0:T(8,128)(2,1)}, bf16[1,128,1024]{2,1,0:T(8,128)(2,1)}, bf16[1,128,1024]{2,1,0:T(8,128)(2,1)}, f32[1,4,512]{2,1,0:T(4,128)}, f32[128,512]{1,0:T(8,128)}) custom-call(bf16[1,128,1024]{2,1,0:T(8,128)(2,1)S(1)} %get-tuple-element.10.refs_0_, bf16[1,128,1024]{2,1,0:T(8,128)(2,1)S(1)} %get-tuple-element.11.refs_1_, ...), custom_call_target="tpu_custom_call" | custom-call | tf_op jit(solution)/shard_map/pallas_call | solution.py:867

commit v2 on v1

--- a/solution.py
+++ b/solution.py
@@ -160,7 +160,7 @@
     q_hbm, k_hbm, v_hbm, o_hbm, cum_hbm, do_hbm, w_hbm,
     dq_out, dk_out, dv_out, dcum_out, dw_out,
     q_ref, k_ref, v_ref, o_ref, cum_ref, dof, wbuf, prob, prob_b, k_t, o_t,
-    dw_part, y_send, y_recv, z_send, z_recv, dw_acc, stage, dcum_ref,
+    dw_part, y_send, y_recv, z_send, z_recv, dw_acc, cot_acc, stage, dcum_ref,
     in_sem, out_sem,
     x_ssem, x_rsem, c_ssem, c_rsem, f_ssem, f_rsem,
     wz_ssem, wz_rsem, wy_ssem, wy_rsem,
@@ -252,7 +252,7 @@
 
     def forward_copy(i, owner_core):
         part = arrived(i, owner_core)
-        return remote(part, part, f_ssem, f_rsem.at[min(i, 1)], sp=core_peer, dp=dp)
+        return remote(part, part, f_ssem, f_rsem.at[i], sp=core_peer, dp=dp)
 
     def x_start():
         loads[0].wait()
@@ -263,18 +263,23 @@
         x_in(i).wait_recv()
         forward_copy(i, core).start()
 
-    chunk_rows = w_rows // w_chunks
+    chunk_cols = width // w_chunks
 
     def w_part(owner_y, c):
-        start = pl.multiple_of(owner_y * w_rows + c * chunk_rows, chunk_rows)
-        return wbuf.at[pl.ds(start, chunk_rows)]
+        rows = pl.ds(pl.multiple_of(owner_y * w_rows, w_rows), w_rows)
+        start = (x * (w_chunks // PAIR) + c) % w_chunks * chunk_cols
+        return wbuf.at[rows, pl.ds(pl.multiple_of(start, chunk_cols), chunk_cols)]
 
     def wz_copy(way, c, target_z):
         return remote(w_part(y, c), w_part(y, c), wz_ssem.at[way], wz_rsem.at[c],
                       sp=sp, dp=target_z * PAIR + y)
 
+    def w_group(c):
+        quarter = c * n_sp // w_chunks
+        return max(quarter - 1, 0) if isinstance(c, int) else jnp.maximum(quarter - 1, 0)
+
     def wy_copy(owner_y, c):
-        return remote(w_part(owner_y, c), w_part(owner_y, c), wy_ssem, wy_rsem,
+        return remote(w_part(owner_y, c), w_part(owner_y, c), wy_ssem, wy_rsem.at[w_group(c)],
                       sp=sp, dp=y_peer)
 
     sends_up = jnp.logical_and(z >= sp, z < n_z - 1)
@@ -398,19 +403,29 @@
     def part_of(step, other):
         return dw_part[2 * step + other]
 
-    def columns_arrive():
-        forward_copy(0, 1 - core).wait_recv()
-        first = pl.multiple_of((1 - x) * PAIR * col_part, PAIR * col_part)
-        part = dof.at[token_rows((1 - x) * PAIR + 1 - core), pl.ds(first, PAIR * col_part)]
-        remote(part, part, f_ssem, f_rsem.at[1], sp=core_peer, dp=dp).wait_recv()
+    def pair_of(turn):
+        return y if turn == 0 else 1 - y
+
+    def columns_arrive(i):
+        forward_copy(i, 1 - core).wait_recv()
+
+    def cot_piece(pair, first, count):
+        start = pl.multiple_of((x * PAIR + first) % n_sp * col_part, col_part)
+        cols = pl.ds(start, count * col_part)
+        return nt(dof[:, cols], wbuf[pl.ds(pl.multiple_of(pair * w_rows, w_rows), w_rows), cols])
+
+    def cot_first():
+        columns_arrive(0)
+        cot_acc[...] = cot_piece(pair_of(0), 0, PAIR)
+
+    def cot_second():
+        columns_arrive(1)
+        cot_acc[...] += cot_piece(pair_of(0), PAIR, 1)
 
     outs = (dq_out, dk_out, dv_out)
 
     def grad_cols(pair):
         return pl.ds(pl.multiple_of(sp * head_cols + pair * LANES, LANES), LANES)
-
-    def pair_of(turn):
-        return y if turn == 0 else 1 - y
 
     def grad_copy(a, turn, off):
         target = (sp + off) % n_sp
@@ -442,15 +457,24 @@
         picks = jnp.where(pick(row, column), 1.0, 0.0).astype(jnp.bfloat16)
         return nt(picks, jnp.concatenate([high, low], axis=1))
 
-    def pair_gradients(turn, early, between):
+    def w_arrives(group):
+        part = wbuf.at[pl.ds(pl.multiple_of((1 - y) * w_rows, w_rows), w_rows),
+                       pl.ds(0, col_part * (1 if group else PAIR))]
+        remote(part, part, wy_ssem, wy_rsem.at[group], sp=sp, dp=y_peer).wait_recv()
+
+    def pair_gradients(turn, early):
         pair = pair_of(turn)
         cols = pair_cols(pair)
-        if turn:
-            block_w = wbuf.at[pl.ds(pl.multiple_of((1 - y) * w_rows, w_rows), w_rows)]
-            remote(block_w, block_w, wy_ssem, wy_rsem, sp=sp, dp=y_peer).wait_recv()
         with ns(f"pair{turn}a0"):
-            pair_w = wbuf[pl.ds(pl.multiple_of(pair * w_rows, w_rows), w_rows), :]
-            cot = nt(dof[...], pair_w).astype(jnp.bfloat16)
+            if turn:
+                w_arrives(0)
+                cot_acc[...] = cot_piece(pair, 0, PAIR)
+                w_arrives(1)
+                cot_acc[...] += cot_piece(pair, PAIR, 1)
+                with ns("wy_wait"):
+                    w_arrives(2)
+            total = cot_acc[...] + cot_piece(pair, n_sp - 1, 1)
+            cot = total.astype(jnp.bfloat16)
             cots = [jnp.where(head_mask(sub), cot, 0) for sub in range(per_pair)]
         with ns(f"pair{turn}a1"):
             value_total = [None] * n_blocks
@@ -487,8 +511,6 @@
                 query_sums = jnp.concatenate(query_parts, axis=1)
                 query_total.append(query_sums[:head_width])
                 row_sums.append(query_sums[head_width:head_width + 1])
-            if sub == 0:
-                between()
         with ns(f"pair{turn}c"):
             first = head_mask(0)
             key_grad = jnp.where(first, key_totals[0], key_totals[1])
@@ -535,22 +557,29 @@
         for c in range(first, last):
             w_later(c, ahead3)
 
+    def far_block(n):
+        return (2, 5 - n) if n >= 4 else (n % 2, 1 - n // 2)
+
     def far_near(n):
+        step, other = far_block(n)
+        value = product(step, other)
+
+        @at_step(3)
+        def _():
+            to_z(n, value, (0, 1, 2, 3, 7, 4)[n], 2)
+
+        @at_step(2)
+        def _():
+            dw_part[2 * step + other] = value
+
+    def pass_on(n):
         step, other = n % 2, 1 - n // 2
-        value = product(step, other)
-
-        @at_step(3)
-        def _():
-            to_z(n, value, n, 2)
-
-        @at_step(2)
-        def _():
-            dw_part[2 * step + other] = value
+        to_z(n, part_of(step, other) + from_z(n), 1 - other, step)
 
     def far_cross(slot, step):
         y_send[slot] = product(step, 1).astype(jnp.bfloat16)
 
-    ahead2 = jnp.where(x == 0, core * w_chunks, 2)
+    ahead2 = jnp.where(x == 0, core * w_chunks, 3 - core)
     ahead3 = jnp.where(x == 0, core * w_chunks, 0)
 
     with ns("b_relay"):
@@ -590,11 +619,13 @@
             to_z(0, product(sibling, 1), 2, sibling)
             to_z(1, product(sibling, 0), 3, sibling)
             keep(3, 0)
-            forward_step(1)
             keep(2, 0)
             keep(step_of, 1)
             keep(step_of, 0)
+            cot_first()
+            forward_step(1)
             forward_step(2)
+            cot_second()
 
         @at_step(2)
         def _():
@@ -609,54 +640,54 @@
             relay2(4, 5)
             far_cross(0, 3)
             relay2(5, 6)
-            far_cross(1, 2)
+            keep(2, 1)
             relay2(6, 7)
             keep(3, 0)
             relay2(7, 8)
             forward_step(1)
             y_copy(0).start()
+            keep(2, 0)
+            cot_first()
+            forward_step(2)
+            pass_on(0)
+            cot_second()
+
+        @at_step(3)
+        def _():
+            for n in range(6):
+                far_near(n)
+            relay3(0, 2)
+            far_cross(1, 3)
+
+            @pl.when(x == 0)
+            def _():
+                forward_step(1)
+
+            relay3(2, 4)
+            keep(3, 0)
+
+            @pl.when(x == 1)
+            def _():
+                forward_step(1)
+
+            @pl.when(x <= core)
+            def _():
+                forward_step(2)
+
+            relay3(4, 6)
+
+            @pl.when(x > core)
+            def _():
+                forward_step(2)
+
+            cot_first()
+            relay3(6, 7)
+            cot_second()
+            relay3(7, 8)
             y_copy(1).start()
-            keep(2, 0)
-            forward_step(2)
-
-        @at_step(3)
-        def _():
-            for n in range(4):
-                far_near(n)
-
-            relay3(0, 2)
-            far_cross(0, 2)
-
-            @pl.when(x == 0)
-            def _():
-                forward_step(1)
-
-            relay3(2, 4)
-            far_cross(1, 3)
-
-            @pl.when(x == 0)
-            def _():
-                forward_step(2)
-
-            relay3(4, 6)
-            keep(2, 0)
-
-            @pl.when(x == 1)
-            def _():
-                forward_step(1)
-                forward_step(2)
-
-            keep(3, 0)
-            relay3(6, 8)
-            y_copy(0).start()
-            y_copy(1).start()
 
     with ns("e_cols2"):
-        columns_arrive()
-
-    def pass_on(n):
-        step, other = n % 2, 1 - n // 2
-        to_z(n, part_of(step, other) + from_z(n), 1 - other, step)
+        columns_arrive(2)
 
     def near_far(slot, step):
         return part_of(step, 0) + from_y(slot)
@@ -675,9 +706,9 @@
 
         @at_step(2)
         def _():
-            pass_on(0)
-
-    def between0():
+            pass_on(1)
+
+    def early0():
         with ns("g_poll"):
             @at_step(0)
             def _():
@@ -687,11 +718,7 @@
             def _():
                 to_z(3, near_far(1, 2), 6, 2)
 
-            @at_step(2)
-            def _():
-                pass_on(1)
-
-    pair_gradients(0, lambda: None, between0)
+    pair_gradients(0, early0)
     with ns("h_poll"):
         @at_step(2)
         def _():
@@ -699,12 +726,6 @@
             pass_on(3)
 
     def early1():
-        with ns("i0_poll"):
-            @at_step(3)
-            def _():
-                to_z(4, part_of(2, 0) + from_y(0), 4, 2)
-
-    def between1():
         with ns("i_poll"):
             @at_step(0)
             def _():
@@ -718,11 +739,15 @@
             def _():
                 to_z(4, part_of(3, 0) + from_y(0), 4, 3)
 
-    pair_gradients(1, early1, between1)
+    pair_gradients(1, early1)
     with ns("j_poll"):
         @at_step(1)
         def _():
             over_y()
+
+        @at_step(2)
+        def _():
+            to_y(1, part_of(2, 1) + from_z(7))
 
     with ns("k_final"):
         @pl.when(near)
@@ -769,9 +794,14 @@
             sent(y_send, ry_ssem)
             sent(z_send.at[pl.ds(0, 4)], rz_ssem)
 
-        @pl.when(far)
+        @at_step(2)
         def _():
             sent(y_send.at[pl.ds(0, 2)], ry_ssem)
+            sent(z_send.at[pl.ds(0, 5)], rz_ssem)
+
+        @at_step(3)
+        def _():
+            sent(y_send.at[pl.ds(0, 1)], ry_ssem)
             sent(z_send, rz_ssem)
 
         sent(rest, g_ssem)
@@ -849,15 +879,16 @@
             pltpu.VMEM((PAIR * n_z, w_rows, col_part), f32),
             pltpu.VMEM((3, w_rows, col_part), bf16),
             pltpu.VMEM((3, w_rows, col_part), bf16),
-            pltpu.VMEM((5, w_rows, col_part), bf16),
-            pltpu.VMEM((7, w_rows, col_part), bf16),
+            pltpu.VMEM((6, w_rows, col_part), bf16),
+            pltpu.VMEM((8, w_rows, col_part), bf16),
             pltpu.VMEM((w_rows, col_part), f32),
+            pltpu.VMEM((length, LANES), f32),
             pltpu.VMEM((3, length, head_cols), bf16),
             pltpu.VMEM(cum.shape[1:], f32),
             dma((7,)), dma((2,)),
-            dma, dma((n_sp - 1,)), dma, dma, dma, dma((PAIR,)),
-            dma((2,)), dma((w_chunks,)), dma, dma,
-            dma, dma((3,)), dma, dma((7,)),
+            dma, dma((n_sp - 1,)), dma, dma, dma, dma((n_sp - 1,)),
+            dma((2,)), dma((w_chunks,)), dma, dma((n_sp - 1,)),
+            dma, dma((3,)), dma, dma((8,)),
             dma, dma, dma,
         ],
         compiler_params=pltpu.CompilerParams(

time: 37.4 us -> 35.1 us (0.939)
  Pallas kernels: 36.6 us -> 34.3 us
    pallas_call x1, Pallas kernels: 35.6 us -> 33.3 us  [fused_shards(): pl.pallas_call(functools.partial(kernel, n_sp, n_dp, n_heads, w_chunks),...]
where the time goes in v2:
time: 35.1 us; the launch traced here: 34.9 us
  Pallas kernels  34.3 us (98%)
  between operations  0.64 us (2%)
    pallas_call x1, Pallas kernels, fused_shards(): pl.pallas_call(functools.partial(kernel, n_sp, n_dp, n_heads, w_chunks),...  33.3 us
    pallas_call x1, Pallas kernels, fused_shards(): pl.pallas_call(hand_over, out_shape=[jax.ShapeDtypeStruct(part.shape, par...  1.01 us

profile of v2, /device:TPU:0, one launch (start us, length us, event | category | flops | bytes accessed | tf_op | source)
XLA Modules:
  0.0 34.9 jit_solution(1278053445830933890)
XLA Ops:
  0.6 33.3 %shard_map.110 = (bf16[1,128,1024]{2,1,0:T(8,128)(2,1)S(1)}, bf16[1,128,1024]{2,1,0:T(8,128)(2,1)S(1)}, bf16[1,128,1024]{2,1,0:T(8,128)(2,1)S(1)}, f32[1,4,512]{2,1,0:T(4,128)S(1)}, f32[128,512]{1,0:T(8,128)S(1)}) custom-call(bf16[1,512,256]{2,1,0:T(8,128)(2,1)} %q_hbm.1, bf16[1,512,256]{2,1,0:T(8,128)(2,1)} %k_hbm.1, bf16[1,512,256]{2,1,0:T(8,128)(2,1)} %v_hbm.1, ...), custom_call_target="tpu_custom_call" | custom-call | tf_op jit(solution)/shard_map/pallas_call | solution.py:858
  33.9 1.0 %shard_map.111 = (bf16[1,128,1024]{2,1,0:T(8,128)(2,1)}, bf16[1,128,1024]{2,1,0:T(8,128)(2,1)}, bf16[1,128,1024]{2,1,0:T(8,128)(2,1)}, f32[1,4,512]{2,1,0:T(4,128)}, f32[128,512]{1,0:T(8,128)}) custom-call(bf16[1,128,1024]{2,1,0:T(8,128)(2,1)S(1)} %get-tuple-element.10.refs_0_, bf16[1,128,1024]{2,1,0:T(8,128)(2,1)S(1)} %get-tuple-element.11.refs_1_, ...), custom_call_target="tpu_custom_call" | custom-call | tf_op jit(solution)/shard_map/pallas_call | solution.py:898

commit v3 on v2

--- a/solution.py
+++ b/solution.py
@@ -165,7 +165,7 @@
     x_ssem, x_rsem, c_ssem, c_rsem, f_ssem, f_rsem,
     wz_ssem, wz_rsem, wy_ssem, wy_rsem,
     ry_ssem, ry_rsem, rz_ssem, rz_rsem,
-    g_ssem, g_rsem, g_lsem,
+    g_ssem, g_rsem, g_lsem, met_sem,
 ):
     sp, dp = lax.axis_index("sp"), lax.axis_index("dp")
     n_z = n_dp // PAIR
@@ -220,13 +220,21 @@
         pl.semaphore_signal(
             barrier, inc=1, device_id={"sp": (sp + off) % n_sp, "dp": dp}, device_id_type=MESH
         )
-    for off in range(1, n_z):
-        pl.semaphore_signal(
-            barrier, inc=1,
-            device_id={"sp": sp, "dp": ((z + off) % n_z) * PAIR + y}, device_id_type=MESH,
-        )
+    neighbours = ((z > 0, z - 1), (z < n_z - 1, z + 1))
+    n_neighbours = sum(jnp.where(there, 1, 0) for there, _ in neighbours)
+
+    def greet(sem):
+        for there, at in neighbours:
+            @pl.when(there)
+            def _():
+                pl.semaphore_signal(
+                    sem, inc=1, device_id={"sp": sp, "dp": at * PAIR + y}, device_id_type=MESH
+                )
+
+    greet(barrier)
     pl.semaphore_signal(barrier, inc=1, device_id={"sp": sp, "dp": y_peer}, device_id_type=MESH)
-    pl.semaphore_wait(barrier, n_sp + n_z - 1)
+    pl.semaphore_wait(barrier, n_sp + n_neighbours)
+    greet(met_sem)
 
     def chip_rows(owner_x):
         return pl.ds(pl.multiple_of(owner_x * PAIR * tokens, PAIR * tokens), PAIR * tokens)
@@ -263,11 +271,12 @@
         x_in(i).wait_recv()
         forward_copy(i, core).start()
 
-    chunk_cols = width // w_chunks
+    w_pieces = PAIR * w_chunks
+    chunk_cols = width // w_pieces
 
     def w_part(owner_y, c):
         rows = pl.ds(pl.multiple_of(owner_y * w_rows, w_rows), w_rows)
-        start = (x * (w_chunks // PAIR) + c) % w_chunks * chunk_cols
+        start = (x * w_chunks + c) % w_pieces * chunk_cols
         return wbuf.at[rows, pl.ds(pl.multiple_of(start, chunk_cols), chunk_cols)]
 
     def wz_copy(way, c, target_z):
@@ -275,7 +284,7 @@
                       sp=sp, dp=target_z * PAIR + y)
 
     def w_group(c):
-        quarter = c * n_sp // w_chunks
+        quarter = c * n_sp // w_pieces
         return max(quarter - 1, 0) if isinstance(c, int) else jnp.maximum(quarter - 1, 0)
 
     def wy_copy(owner_y, c):
@@ -299,28 +308,32 @@
 
     near = z // PAIR == x
     far = z // PAIR != x
-    held = w_chunks - 2
+    held = w_chunks - 3
 
     @pl.when(z == sp)
     def _():
         w_load.wait()
-        for c in range(w_chunks):
-            w_send(c)
+        for p in range(w_pieces):
+            w_send(p)
         x_start()
-        for c in range(held):
-            w_cross(c)
+        for p in range(PAIR * held):
+            w_cross(p)
 
     @pl.when(z != sp)
     def _():
         x_start()
 
+    def pieces_of(c):
+        return [PAIR * c + i for i in range(PAIR)]
+
     def w_step(c, cross=True):
         @pl.when(z != sp)
         def _():
-            wz_copy(0, c, z).wait_recv()
-            w_send(c)
-            if cross:
-                w_cross(c)
+            for p in pieces_of(c):
+                wz_copy(0, p, z).wait_recv()
+                w_send(p)
+                if cross:
+                    w_cross(p)
 
     lane = lax.broadcasted_iota(jnp.int32, (1, LANES), 1)
 
@@ -427,8 +440,7 @@
     def grad_cols(pair):
         return pl.ds(pl.multiple_of(sp * head_cols + pair * LANES, LANES), LANES)
 
-    def grad_copy(a, turn, off):
-        target = (sp + off) % n_sp
+    def grad_copy(a, turn, target):
         pair = pair_of(turn)
         return remote(stage.at[a, token_rows(target), pair_cols(pair)],
                       outs[a].at[0, :, grad_cols(pair)],
@@ -444,9 +456,12 @@
             piece = part[b * block:(b + 1) * block]
             totals[b] = piece if totals[b] is None else totals[b] + piece
 
-    def send_grad(a, turn):
-        for off in range(1, n_sp):
-            grad_copy(a, turn, off).start()
+    def send_away(a, turn):
+        for i in range(PAIR):
+            grad_copy(a, turn, (1 - x) * PAIR + i).start()
+
+    def send_home(a, turn):
+        grad_copy(a, turn, core_peer).start()
         grad_keep(a, turn).start()
 
     def picked(left, pick):
@@ -461,6 +476,59 @@
         part = wbuf.at[pl.ds(pl.multiple_of((1 - y) * w_rows, w_rows), w_rows),
                        pl.ds(0, col_part * (1 if group else PAIR))]
         remote(part, part, wy_ssem, wy_rsem.at[group], sp=sp, dp=y_peer).wait_recv()
+
+    def score_gradients(turn, cot, cots, side):
+        away = 1 - side
+        pair = pair_of(turn)
+        cols = pair_cols(pair)
+        values = v_ref[:, cols]
+        with ns(f"pair{turn}a2"):
+            own_out = o_ref[:, grad_cols(pair)]
+            dots = picked(cot.astype(jnp.float32) * own_out.astype(jnp.float32),
+                          lambda row, column: column // head_width == row)
+        queries, keys_ts = [], []
+        for sub in range(per_pair):
+            h = pair * per_pair + sub
+            spare = jnp.where(lane == (1 - sub) * head_width, 1.0, 0.0).astype(jnp.bfloat16)
+            queries.append(jnp.where(head_mask(sub), q_ref[:, cols], spare))
+            keys_t = k_t[pl.ds(pl.multiple_of(h * head_width, head_width), head_width), :]
+            keys_ts.append(
+                jnp.concatenate([keys_t, jnp.ones((16, length), jnp.bfloat16)], axis=0))
+        key_totals = [[None] * n_blocks for _ in range(per_pair)]
+        row_sums = [[None] * n_blocks for _ in range(per_pair)]
+        first = head_mask(0)
+
+        def finish_keys(b):
+            total = jnp.where(first, key_totals[0][b], key_totals[1][b])
+            stage[1, b * block:(b + 1) * block, cols] = (total * scale).astype(jnp.bfloat16)
+            (send_away if b == away else send_home)(1, turn)
+
+        for b in (away, side):
+            with ns(f"pair{turn}b{int(b == side)}"):
+                lo, end = b * block, (b + 1) * block
+                query_parts = []
+                for sub in range(per_pair):
+                    weights = prob[pair * per_pair + sub, :end, lo:end]
+                    d_prob = nt(values[:end], cots[sub][lo:end])
+                    score_b = (weights * (d_prob - dots[sub:sub + 1, lo:end])).astype(jnp.bfloat16)
+                    add_rows(key_totals[sub], nn(score_b, queries[sub][lo:end]))
+                    query_sums = nn(keys_ts[sub][:, :end], score_b)
+                    query_parts.append(query_sums[:head_width])
+                    row_sums[sub][b] = query_sums[head_width:head_width + 1]
+                if b == n_blocks - 1:
+                    finish_keys(away)
+                query_grad = jnp.concatenate(query_parts, axis=0).T * scale
+                stage[0, lo:end, cols] = query_grad.astype(jnp.bfloat16)
+                (send_away if b == away else send_home)(0, turn)
+        with ns(f"pair{turn}c"):
+            finish_keys(side)
+            spare_sums = [jnp.where(first, key_totals[1][b], key_totals[0][b])
+                          for b in range(n_blocks)]
+            col_sums = picked(jnp.concatenate(spare_sums, axis=0),
+                              lambda row, column: column == (1 - row) * head_width)
+            for sub in range(per_pair):
+                d_cum = jnp.concatenate(row_sums[sub], axis=1) - col_sums[sub:sub + 1]
+                dcum_ref[pl.ds(pair * per_pair + sub, 1), :] = d_cum
 
     def pair_gradients(turn, early):
         pair = pair_of(turn)
@@ -484,45 +552,13 @@
                     lo, end = b * block, (b + 1) * block
                     add_rows(value_total, nn(prob_b[h, :end, lo:end], cots[sub][lo:end]))
             stage[2, :, cols] = jnp.concatenate(value_total, axis=0).astype(jnp.bfloat16)
-            send_grad(2, turn)
+            send_away(2, turn)
+            send_home(2, turn)
         early()
-        with ns(f"pair{turn}a2"):
-            own_out = o_ref[:, grad_cols(pair)]
-            values = v_ref[:, cols]
-            dots = picked(cot.astype(jnp.float32) * own_out.astype(jnp.float32),
-                          lambda row, column: column // head_width == row)
-        key_totals, query_total, row_sums = [], [], []
-        for sub in range(per_pair):
-            with ns(f"pair{turn}b{sub}"):
-                h = pair * per_pair + sub
-                spare = jnp.where(lane == (1 - sub) * head_width, 1.0, 0.0).astype(jnp.bfloat16)
-                query_h = jnp.where(head_mask(sub), q_ref[:, cols], spare)
-                keys_t = k_t[pl.ds(pl.multiple_of(h * head_width, head_width), head_width), :]
-                keys_t = jnp.concatenate([keys_t, jnp.ones((16, length), jnp.bfloat16)], axis=0)
-                key_total, query_parts = [None] * n_blocks, []
-                for b in range(n_blocks):
-                    lo, end = b * block, (b + 1) * block
-                    weights = prob[h, :end, lo:end]
-                    d_prob = nt(values[:end], cots[sub][lo:end])
-                    score_b = (weights * (d_prob - dots[sub:sub + 1, lo:end])).astype(jnp.bfloat16)
-                    add_rows(key_total, nn(score_b, query_h[lo:end]))
-                    query_parts.append(nn(keys_t[:, :end], score_b))
-                key_totals.append(jnp.concatenate(key_total, axis=0))
-                query_sums = jnp.concatenate(query_parts, axis=1)
-                query_total.append(query_sums[:head_width])
-                row_sums.append(query_sums[head_width:head_width + 1])
-        with ns(f"pair{turn}c"):
-            first = head_mask(0)
-            key_grad = jnp.where(first, key_totals[0], key_totals[1])
-            stage[1, :, cols] = (key_grad * scale).astype(jnp.bfloat16)
-            send_grad(1, turn)
-            stage[0, :, cols] = (jnp.concatenate(query_total, axis=0).T * scale).astype(jnp.bfloat16)
-            send_grad(0, turn)
-            col_sums = picked(jnp.where(first, key_totals[1], key_totals[0]),
-                              lambda row, column: column == (1 - row) * head_width)
-            for sub in range(per_pair):
-                d_cum = row_sums[sub] - col_sums[sub:sub + 1]
-                dcum_ref[pl.ds(pair * per_pair + sub, 1), :] = d_cum
+        for side in range(PAIR):
+            @pl.when(x == side)
+            def _():
+                score_gradients(turn, cot, cots, side)
 
     def at_step(step):
         return lambda action: pl.when(step_of == step)(action)
@@ -534,6 +570,8 @@
         for h in range(n_heads):
             probabilities(h)
 
+    pl.semaphore_wait(met_sem, n_neighbours)
+
     def relay(first, last):
         for c in range(first, last):
             w_step(c)
@@ -558,7 +596,7 @@
             w_later(c, ahead3)
 
     def far_block(n):
-        return (2, 5 - n) if n >= 4 else (n % 2, 1 - n // 2)
+        return (2, 5 - n) if isinstance(n, int) and n >= 4 else (n % 2, 1 - n // 2)
 
     def far_near(n):
         step, other = far_block(n)
@@ -582,6 +620,8 @@
     ahead2 = jnp.where(x == 0, core * w_chunks, 3 - core)
     ahead3 = jnp.where(x == 0, core * w_chunks, 0)
 
+    late3 = jnp.logical_and(x == 0, core == 1)
+
     with ns("b_relay"):
         @pl.when(near)
         def _():
@@ -606,7 +646,7 @@
 
         @at_step(3)
         def _():
-            columns_first(ahead3)
+            columns_first(jnp.where(late3, 4, ahead3))
 
     with ns("d_dw"):
         @pl.when(near)
@@ -614,8 +654,8 @@
             sibling = 1 - step_of
             to_y(0, product(3, 1))
             to_y(1, product(2, 1))
-            for c in range(held, w_chunks):
-                w_cross(c)
+            for p in range(PAIR * held, w_pieces):
+                w_cross(p)
             to_z(0, product(sibling, 1), 2, sibling)
             to_z(1, product(sibling, 0), 3, sibling)
             keep(3, 0)
@@ -638,24 +678,32 @@
             relay2(3, 4)
             far_near(3)
             relay2(4, 5)
-            far_cross(0, 3)
+            to_y(0, product(3, 1))
             relay2(5, 6)
             keep(2, 1)
             relay2(6, 7)
             keep(3, 0)
             relay2(7, 8)
             forward_step(1)
-            y_copy(0).start()
             keep(2, 0)
             cot_first()
             forward_step(2)
-            pass_on(0)
+
+            @pl.when(core == 0)
+            def _():
+                pass_on(0)
+
             cot_second()
 
         @at_step(3)
         def _():
             for n in range(6):
                 far_near(n)
+                if n < 4:
+                    @pl.when(late3)
+                    def _():
+                        w_step(n + 4)
+
             relay3(0, 2)
             far_cross(1, 3)
 
@@ -684,7 +732,6 @@
             relay3(6, 7)
             cot_second()
             relay3(7, 8)
-            y_copy(1).start()
 
     with ns("e_cols2"):
         columns_arrive(2)
@@ -692,6 +739,9 @@
     def near_far(slot, step):
         return part_of(step, 0) + from_y(slot)
 
+    def far_over_y():
+        to_y(1, part_of(2, 1) + from_z(7))
+
     def over_y():
         to_y(2, part_of(step_of, 1) + from_z(0) + from_z(2))
 
@@ -706,7 +756,7 @@
 
         @at_step(2)
         def _():
-            pass_on(1)
+            pass_on(1 - core)
 
     def early0():
         with ns("g_poll"):
@@ -718,12 +768,20 @@
             def _():
                 to_z(3, near_far(1, 2), 6, 2)
 
+            @at_step(2)
+            def _():
+                pass_on(2 - core)
+
     pair_gradients(0, early0)
     with ns("h_poll"):
         @at_step(2)
         def _():
-            pass_on(2)
-            pass_on(3)
+            to_z(4, part_of(3, 0) + from_y(0), 4, 3)
+            pass_on(3 - core)
+
+        @at_step(3)
+        def _():
+            y_copy(1).start()
 
     def early1():
         with ns("i_poll"):
@@ -734,20 +792,23 @@
             @at_step(1)
             def _():
                 to_z(2, part_of(3, 0) + from_z(4), 5, 3)
+                over_y()
 
             @at_step(2)
             def _():
-                to_z(4, part_of(3, 0) + from_y(0), 4, 3)
+                @pl.when(core == 0)
+                def _():
+                    far_over_y()
+
+                @pl.when(core == 1)
+                def _():
+                    pass_on(3)
 
     pair_gradients(1, early1)
     with ns("j_poll"):
-        @at_step(1)
-        def _():
-            over_y()
-
-        @at_step(2)
-        def _():
-            to_y(1, part_of(2, 1) + from_z(7))
+        @pl.when(jnp.logical_and(step_of == 2, core == 1))
+        def _():
+            far_over_y()
 
     with ns("k_final"):
         @pl.when(near)
@@ -832,7 +893,7 @@
     w_rows = w_out.shape[0] // n_dp
     if head_cols % LANES or n_heads == 0 or 8 % n_heads:
         return False
-    if LANES != PAIR * (head_cols // n_heads) or length % (2 * LANES) or (width // n_sp) % LANES:
+    if LANES != PAIR * (head_cols // n_heads) or length != PAIR * 2 * LANES or (width // n_sp) % LANES:
         return False
     if n_sp & (n_sp - 1) or n_sp < PAIR or n_dp != PAIR * n_sp or n_sp != PAIR * PAIR or head_cols != PAIR * LANES or w_rows != LANES:
         return False
@@ -887,9 +948,9 @@
             pltpu.VMEM(cum.shape[1:], f32),
             dma((7,)), dma((2,)),
             dma, dma((n_sp - 1,)), dma, dma, dma, dma((n_sp - 1,)),
-            dma((2,)), dma((w_chunks,)), dma, dma((n_sp - 1,)),
+            dma((2,)), dma((PAIR * w_chunks,)), dma, dma((n_sp - 1,)),
             dma, dma((3,)), dma, dma((8,)),
-            dma, dma, dma,
+            dma, dma, dma, pltpu.SemaphoreType.REGULAR,
         ],
         compiler_params=pltpu.CompilerParams(
             collective_id=0, has_side_effects=True, vmem_limit_bytes=48 * 2**20

time: 35.1 us -> 34 us (0.969)
  Pallas kernels: 34.3 us -> 33.1 us
    pallas_call x1, Pallas kernels: 33.3 us -> 32 us  [fused_shards(): pl.pallas_call(functools.partial(kernel, n_sp, n_dp, n_heads, w_chunks),...]
where the time goes in v3:
time: 34 us; the launch traced here: 33.9 us
  Pallas kernels  33.1 us (97%)
  between operations  0.8 us (2%)
    pallas_call x1, Pallas kernels, fused_shards(): pl.pallas_call(functools.partial(kernel, n_sp, n_dp, n_heads, w_chunks),...  32 us
    pallas_call x1, Pallas kernels, fused_shards(): pl.pallas_call(hand_over, out_shape=[jax.ShapeDtypeStruct(part.shape, par...  1.01 us

profile of v3, /device:TPU:0, one launch (start us, length us, event | category | flops | bytes accessed | tf_op | source)
XLA Modules:
  0.0 33.9 jit_solution(8155246039365735634)
XLA Ops:
  0.6 32.0 %shard_map.110 = (bf16[1,128,1024]{2,1,0:T(8,128)(2,1)S(1)}, bf16[1,128,1024]{2,1,0:T(8,128)(2,1)S(1)}, bf16[1,128,1024]{2,1,0:T(8,128)(2,1)S(1)}, f32[1,4,512]{2,1,0:T(4,128)S(1)}, f32[128,512]{1,0:T(8,128)S(1)}) custom-call(bf16[1,512,256]{2,1,0:T(8,128)(2,1)} %q_hbm.1, bf16[1,512,256]{2,1,0:T(8,128)(2,1)} %k_hbm.1, bf16[1,512,256]{2,1,0:T(8,128)(2,1)} %v_hbm.1, ...), custom_call_target="tpu_custom_call" | custom-call | tf_op jit(solution)/shard_map/pallas_call | solution.py:919
  32.7 1.0 %shard_map.111 = (bf16[1,128,1024]{2,1,0:T(8,128)(2,1)}, bf16[1,128,1024]{2,1,0:T(8,128)(2,1)}, bf16[1,128,1024]{2,1,0:T(8,128)(2,1)}, f32[1,4,512]{2,1,0:T(4,128)}, f32[128,512]{1,0:T(8,128)}) custom-call(bf16[1,128,1024]{2,1,0:T(8,128)(2,1)S(1)} %get-tuple-element.10.refs_0_, bf16[1,128,1024]{2,1,0:T(8,128)(2,1)S(1)} %get-tuple-element.11.refs_1_, ...), custom_call_target="tpu_custom_call" | custom-call | tf_op jit(solution)/shard_map/pallas_call | solution.py:959

commit v4 on v3

--- a/solution.py
+++ b/solution.py
@@ -166,6 +166,7 @@
     wz_ssem, wz_rsem, wy_ssem, wy_rsem,
     ry_ssem, ry_rsem, rz_ssem, rz_rsem,
     g_ssem, g_rsem, g_lsem, met_sem,
+    detour, det_ssem, det_rsem,
 ):
     sp, dp = lax.axis_index("sp"), lax.axis_index("dp")
     n_z = n_dp // PAIR
@@ -214,6 +215,13 @@
 
     for load in loads[1:]:
         load.start()
+    detour_cols = pl.ds(pl.multiple_of((PAIR + n_sp - 1) % n_sp * col_part, col_part), col_part)
+
+    def detour_load():
+        return pltpu.make_async_copy(w_hbm.at[:, detour_cols], detour, in_sem.at[7])
+
+    begins = jnp.logical_and(x == 0, z == PAIR + core)
+    pl.when(begins)(detour_load().start)
 
     barrier = pltpu.get_barrier_semaphore()
     for off in range(1, n_sp):
@@ -291,6 +299,38 @@
         return remote(w_part(owner_y, c), w_part(owner_y, c), wy_ssem, wy_rsem.at[w_group(c)],
                       sp=sp, dp=y_peer)
 
+    detour_from = w_pieces - w_pieces // n_sp
+    skips = jnp.logical_and(x == 1, z == 1)
+    detour_rows = pl.ds(pl.multiple_of(y * w_rows, w_rows), w_rows)
+
+    def on(here_z, here_core):
+        return jnp.logical_and(x == 0, jnp.logical_and(z == here_z, core == here_core))
+
+    def detour_copy(to_sp, to_z, inside=True):
+        target = detour if inside else wbuf.at[detour_rows, detour_cols]
+        return remote(detour, target, det_ssem, det_rsem, sp=to_sp, dp=to_z * PAIR + y)
+
+    def detour_first(to_z):
+        def run():
+            detour_load().wait()
+            detour_copy(sp, to_z).start()
+
+        return run
+
+    def detour_relay():
+        detour_copy(sp, 0).wait_recv()
+        detour_copy(sp, 0).start()
+
+    def detour_cross():
+        detour_copy(sp, 0).wait_recv()
+        detour_copy(PAIR + core, 0, False).start()
+
+    def detour_take():
+        part = wbuf.at[detour_rows, detour_cols]
+        remote(part, part, det_ssem, det_rsem, sp=core_peer, dp=dp).wait_recv()
+        for p in range(detour_from, w_pieces):
+            w_cross(p)
+
     sends_up = jnp.logical_and(z >= sp, z < n_z - 1)
     sends_down = jnp.logical_and(z <= sp, z > 0)
 
@@ -299,7 +339,9 @@
         def _():
             wz_copy(0, c, z + 1).start()
 
-        @pl.when(sends_down)
+        skip = jnp.logical_and(skips, c >= detour_from)
+
+        @pl.when(jnp.logical_and(sends_down, jnp.logical_not(skip)))
         def _():
             wz_copy(1, c, z - 1).start()
 
@@ -571,6 +613,8 @@
             probabilities(h)
 
     pl.semaphore_wait(met_sem, n_neighbours)
+    pl.when(on(PAIR, 0))(detour_first(0))
+    pl.when(on(PAIR + 1, 1))(detour_first(1))
 
     def relay(first, last):
         for c in range(first, last):
@@ -617,7 +661,7 @@
     def far_cross(slot, step):
         y_send[slot] = product(step, 1).astype(jnp.bfloat16)
 
-    ahead2 = jnp.where(x == 0, core * w_chunks, 3 - core)
+    ahead2 = jnp.where(x == 0, core * w_chunks, 3 - 3 * core)
     ahead3 = jnp.where(x == 0, core * w_chunks, 0)
 
     late3 = jnp.logical_and(x == 0, core == 1)
@@ -625,20 +669,37 @@
     with ns("b_relay"):
         @pl.when(near)
         def _():
-            relay(0, 4)
+            def blocks_over_y(between):
+                core_copy(core_peer).wait_recv()
+                to_y(0, product(3, 1))
+                between()
+                to_y(1, product(2, 1))
+
+            def cross_held():
+                for p in range(PAIR * held, w_pieces):
+                    w_cross(p)
+
+            behind = jnp.logical_and(x * core == 1, step_of == 1)
+            pl.when(behind)(lambda: w_step(2))
+            relay(0, 2)
+            pl.when(jnp.logical_not(behind))(lambda: w_step(2))
+            relay(3, 4)
 
             @pl.when(core == 0)
             def _():
                 forward_step(0)
-
-            for c in range(4, w_chunks):
-                w_step(c, c < held)
+                blocks_over_y(lambda: w_step(4))
+                relay(5, w_chunks)
+                pl.when(z == sp)(cross_held)
 
             @pl.when(core == 1)
             def _():
+                for c in range(4, w_chunks):
+                    w_step(c, c < held)
+                pl.when(on(1, 1))(detour_relay)
                 forward_step(0)
-
-            core_copy(core_peer).wait_recv()
+                blocks_over_y(lambda: None)
+                cross_held()
 
         @at_step(2)
         def _():
@@ -652,20 +713,18 @@
         @pl.when(near)
         def _():
             sibling = 1 - step_of
-            to_y(0, product(3, 1))
-            to_y(1, product(2, 1))
-            for p in range(PAIR * held, w_pieces):
-                w_cross(p)
             to_z(0, product(sibling, 1), 2, sibling)
             to_z(1, product(sibling, 0), 3, sibling)
             keep(3, 0)
             keep(2, 0)
             keep(step_of, 1)
             keep(step_of, 0)
+            pl.when(on(0, 0))(detour_cross)
             cot_first()
             forward_step(1)
             forward_step(2)
             cot_second()
+            pl.when(on(0, 1))(detour_cross)
 
         @at_step(2)
         def _():
@@ -680,58 +739,101 @@
             relay2(4, 5)
             to_y(0, product(3, 1))
             relay2(5, 6)
-            keep(2, 1)
-            relay2(6, 7)
+
+            @pl.when(core == 0)
+            def _():
+                pass_on(0)
+                keep(2, 1)
+
+            @pl.when(core == 1)
+            def _():
+                far_cross(1, 2)
+
+
+            @pl.when(x > core)
+            def _():
+                relay2(6, 8)
+
+            forward_step(1)
+            cot_first()
+
+            @pl.when(x <= core)
+            def _():
+                relay2(6, 7)
+
             keep(3, 0)
-            relay2(7, 8)
-            forward_step(1)
+            pl.when(core == 1)(lambda: forward_step(2))
+
+            @pl.when(x <= core)
+            def _():
+                relay2(7, 8)
+
             keep(2, 0)
-            cot_first()
-            forward_step(2)
 
             @pl.when(core == 0)
             def _():
+                pass_on(1)
+                forward_step(2)
+
+
+            @pl.when(core == 1)
+            def _():
                 pass_on(0)
 
             cot_second()
 
         @at_step(3)
         def _():
-            for n in range(6):
+            for n in range(4):
                 far_near(n)
-                if n < 4:
-                    @pl.when(late3)
-                    def _():
-                        w_step(n + 4)
+
+                @pl.when(late3)
+                def _():
+                    w_step(n + 4)
+
+            @pl.when(core == 0)
+            def _():
+                far_near(4)
+                far_near(5)
+
+            @pl.when(core == 1)
+            def _():
+                far_cross(0, 2)
+                keep(2, 0)
 
             relay3(0, 2)
             far_cross(1, 3)
 
-            @pl.when(x == 0)
-            def _():
-                forward_step(1)
-
-            relay3(2, 4)
+            @pl.when(x > core)
+            def _():
+                relay3(2, 5)
+
+            forward_step(1)
+            pl.when(x * core == 1)(lambda: forward_step(2))
+
+            @pl.when(x <= core)
+            def _():
+                relay3(2, 4)
+
             keep(3, 0)
-
-            @pl.when(x == 1)
-            def _():
-                forward_step(1)
+            pl.when(x == 0)(lambda: forward_step(2))
 
             @pl.when(x <= core)
             def _():
-                forward_step(2)
-
-            relay3(4, 6)
-
-            @pl.when(x > core)
-            def _():
-                forward_step(2)
-
+                relay3(4, 5)
+
+            relay3(5, 6)
             cot_first()
-            relay3(6, 7)
+            pl.when(x == 0)(lambda: relay3(6, 7))
+            pl.when(x > core)(lambda: forward_step(2))
+            pl.when(x > core)(detour_take)
             cot_second()
-            relay3(7, 8)
+            pl.when(x * core == 1)(detour_take)
+            pl.when(x == 0)(lambda: relay3(7, 8))
+
+            @pl.when(x * core == 1)
+            def _():
+                y_copy(0).start()
 
     with ns("e_cols2"):
         columns_arrive(2)
@@ -742,6 +844,11 @@
     def far_over_y():
         to_y(1, part_of(2, 1) + from_z(7))
 
+    last1 = jnp.logical_and(step_of == 3, core == 1)
+
+    def last_block():
+        to_z(5, part_of(2, 0) + from_y(0), 4, 2)
+
     def over_y():
         to_y(2, part_of(step_of, 1) + from_z(0) + from_z(2))
 
@@ -753,10 +860,6 @@
         @at_step(1)
         def _():
             dw_part[6] = near_far(0, 3)
-
-        @at_step(2)
-        def _():
-            pass_on(1 - core)
 
     def early0():
         with ns("g_poll"):
@@ -770,18 +873,27 @@
 
             @at_step(2)
             def _():
-                pass_on(2 - core)
+                @pl.when(core == 1)
+                def _():
+                    pass_on(1)
 
     pair_gradients(0, early0)
     with ns("h_poll"):
         @at_step(2)
         def _():
+            pl.when(core == 1)(y_copy(1).start)
             to_z(4, part_of(3, 0) + from_y(0), 4, 3)
-            pass_on(3 - core)
+            pass_on(2)
 
         @at_step(3)
         def _():
-            y_copy(1).start()
+            @pl.when(x < core)
+            def _():
+                y_copy(0).start()
+
+            @pl.when(x == core)
+            def _():
+                y_copy(1).start()
 
     def early1():
         with ns("i_poll"):
@@ -796,19 +908,22 @@
 
             @at_step(2)
             def _():
-                @pl.when(core == 0)
-                def _():
-                    far_over_y()
-
-                @pl.when(core == 1)
-                def _():
-                    pass_on(3)
+                pass_on(3)
+                pl.when(core == 0)(far_over_y)
+
+            @pl.when(last1)
+            def _():
+                pl.when(x == 0)(y_copy(1).start)
+
+            @pl.when(jnp.logical_and(step_of == 3, x > core))
+            def _():
+                y_copy(1).start()
 
     pair_gradients(1, early1)
     with ns("j_poll"):
-        @pl.when(jnp.logical_and(step_of == 2, core == 1))
-        def _():
-            far_over_y()
+        @pl.when(last1)
+        def _():
+            last_block()
 
     with ns("k_final"):
         @pl.when(near)
@@ -846,9 +961,19 @@
         def _():
             sent(block_w, wz_ssem.at[0])
 
-        @pl.when(sends_down)
+        @pl.when(jnp.logical_and(sends_down, jnp.logical_not(skips)))
         def _():
             sent(block_w, wz_ssem.at[1])
+
+        @pl.when(jnp.logical_and(sends_down, skips))
+        def _():
+            sent(wbuf.at[own_w, pl.ds(0, detour_from * chunk_cols)], wz_ssem.at[1])
+
+        detours = (begins, on(1, 1), jnp.logical_and(x == 0, z == 0))
+
+        @pl.when(functools.reduce(jnp.logical_or, detours))
+        def _():
+            sent(detour, det_ssem)
 
         @pl.when(near)
         def _():
@@ -862,8 +987,15 @@
 
         @at_step(3)
         def _():
-            sent(y_send.at[pl.ds(0, 1)], ry_ssem)
-            sent(z_send, rz_ssem)
+            @pl.when(core == 0)
+            def _():
+                sent(y_send.at[pl.ds(0, 1)], ry_ssem)
+                sent(z_send, rz_ssem)
+
+            @pl.when(core == 1)
+            def _():
+                sent(y_send.at[pl.ds(0, 2)], ry_ssem)
+                sent(z_send.at[pl.ds(0, 5)], rz_ssem)
 
         sent(rest, g_ssem)
     with ns("p_gradwait"):
@@ -946,11 +1078,12 @@
             pltpu.VMEM((length, LANES), f32),
             pltpu.VMEM((3, length, head_cols), bf16),
             pltpu.VMEM(cum.shape[1:], f32),
-            dma((7,)), dma((2,)),
+            dma((8,)), dma((2,)),
             dma, dma((n_sp - 1,)), dma, dma, dma, dma((n_sp - 1,)),
             dma((2,)), dma((PAIR * w_chunks,)), dma, dma((n_sp - 1,)),
             dma, dma((3,)), dma, dma((8,)),
             dma, dma, dma, pltpu.SemaphoreType.REGULAR,
+            pltpu.VMEM((w_rows, col_part), bf16), dma, dma,
         ],
         compiler_params=pltpu.CompilerParams(
             collective_id=0, has_side_effects=True, vmem_limit_bytes=48 * 2**20

time: 34 us -> 33.5 us (0.985)
  Pallas kernels: 33.1 us -> 32.6 us
    pallas_call x1, Pallas kernels: 32 us -> 31.5 us  [fused_shards(): pl.pallas_call(functools.partial(kernel, n_sp, n_dp, n_heads, w_chunks),...]
where the time goes in v4:
time: 33.5 us; the launch traced here: 33.4 us
  Pallas kernels  32.6 us (97%)
  between operations  0.8 us (2%)
    pallas_call x1, Pallas kernels, fused_shards(): pl.pallas_call(functools.partial(kernel, n_sp, n_dp, n_heads, w_chunks),...  31.5 us
    pallas_call x1, Pallas kernels, fused_shards(): pl.pallas_call(hand_over, out_shape=[jax.ShapeDtypeStruct(part.shape, par...  1.01 us

profile of v4, /device:TPU:0, one launch (start us, length us, event | category | flops | bytes accessed | tf_op | source)
XLA Modules:
  0.0 33.4 jit_solution(10009407628440283675)
XLA Ops:
  0.6 31.5 %shard_map.110 = (bf16[1,128,1024]{2,1,0:T(8,128)(2,1)S(1)}, bf16[1,128,1024]{2,1,0:T(8,128)(2,1)S(1)}, bf16[1,128,1024]{2,1,0:T(8,128)(2,1)S(1)}, f32[1,4,512]{2,1,0:T(4,128)S(1)}, f32[128,512]{1,0:T(8,128)S(1)}) custom-call(bf16[1,512,256]{2,1,0:T(8,128)(2,1)} %q_hbm.1, bf16[1,512,256]{2,1,0:T(8,128)(2,1)} %k_hbm.1, bf16[1,512,256]{2,1,0:T(8,128)(2,1)} %v_hbm.1, ...), custom_call_target="tpu_custom_call" | custom-call | tf_op jit(solution)/shard_map/pallas_call | solution.py:1051
  32.2 1.0 %shard_map.111 = (bf16[1,128,1024]{2,1,0:T(8,128)(2,1)}, bf16[1,128,1024]{2,1,0:T(8,128)(2,1)}, bf16[1,128,1024]{2,1,0:T(8,128)(2,1)}, f32[1,4,512]{2,1,0:T(4,128)}, f32[128,512]{1,0:T(8,128)}) custom-call(bf16[1,128,1024]{2,1,0:T(8,128)(2,1)S(1)} %get-tuple-element.10.refs_0_, bf16[1,128,1024]{2,1,0:T(8,128)(2,1)S(1)} %get-tuple-element.11.refs_1_, ...), custom_call_target="tpu_custom_call" | custom-call | tf_op jit(solution)/shard_map/pallas_call | solution.py:1092

commit v5 on v4

--- a/solution.py
+++ b/solution.py
@@ -586,20 +586,23 @@
             total = cot_acc[...] + cot_piece(pair, n_sp - 1, 1)
             cot = total.astype(jnp.bfloat16)
             cots = [jnp.where(head_mask(sub), cot, 0) for sub in range(per_pair)]
-        with ns(f"pair{turn}a1"):
-            value_total = [None] * n_blocks
-            for sub in range(per_pair):
-                h = pair * per_pair + sub
-                for b in range(n_blocks):
-                    lo, end = b * block, (b + 1) * block
-                    add_rows(value_total, nn(prob_b[h, :end, lo:end], cots[sub][lo:end]))
-            stage[2, :, cols] = jnp.concatenate(value_total, axis=0).astype(jnp.bfloat16)
-            send_away(2, turn)
-            send_home(2, turn)
+        def value_gradients():
+            with ns(f"pair{turn}a1"):
+                value_total = [None] * n_blocks
+                for sub in range(per_pair):
+                    h = pair * per_pair + sub
+                    for b in range(n_blocks):
+                        lo, end = b * block, (b + 1) * block
+                        add_rows(value_total, nn(prob_b[h, :end, lo:end], cots[sub][lo:end]))
+                stage[2, :, cols] = jnp.concatenate(value_total, axis=0).astype(jnp.bfloat16)
+                send_away(2, turn)
+                send_home(2, turn)
+
         early()
         for side in range(PAIR):
             @pl.when(x == side)
             def _():
+                value_gradients()
                 score_gradients(turn, cot, cots, side)
 
     def at_step(step):

time: 33.5 us -> 33.3 us (level)
  no operation moved by 1% of the time
where the time goes in v5:
time: 33.3 us; the launch traced here: 33.2 us
  Pallas kernels  32.4 us (97%)
  between operations  0.8 us (2%)
    pallas_call x1, Pallas kernels, fused_shards(): pl.pallas_call(functools.partial(kernel, n_sp, n_dp, n_heads, w_chunks),...  31.4 us
    pallas_call x1, Pallas kernels, fused_shards(): pl.pallas_call(hand_over, out_shape=[jax.ShapeDtypeStruct(part.shape, par...  1.01 us

profile of v5, /device:TPU:0, one launch (start us, length us, event | category | flops | bytes accessed | tf_op | source)
XLA Modules:
  0.0 33.2 jit_solution(12055710430357927869)
XLA Ops:
  0.6 31.4 %shard_map.110 = (bf16[1,128,1024]{2,1,0:T(8,128)(2,1)S(1)}, bf16[1,128,1024]{2,1,0:T(8,128)(2,1)S(1)}, bf16[1,128,1024]{2,1,0:T(8,128)(2,1)S(1)}, f32[1,4,512]{2,1,0:T(4,128)S(1)}, f32[128,512]{1,0:T(8,128)S(1)}) custom-call(bf16[1,512,256]{2,1,0:T(8,128)(2,1)} %q_hbm.1, bf16[1,512,256]{2,1,0:T(8,128)(2,1)} %k_hbm.1, bf16[1,512,256]{2,1,0:T(8,128)(2,1)} %v_hbm.1, ...), custom_call_target="tpu_custom_call" | custom-call | tf_op jit(solution)/shard_map/pallas_call | solution.py:1054
  32.0 1.0 %shard_map.111 = (bf16[1,128,1024]{2,1,0:T(8,128)(2,1)}, bf16[1,128,1024]{2,1,0:T(8,128)(2,1)}, bf16[1,128,1024]{2,1,0:T(8,128)(2,1)}, f32[1,4,512]{2,1,0:T(4,128)}, f32[128,512]{1,0:T(8,128)}) custom-call(bf16[1,128,1024]{2,1,0:T(8,128)(2,1)S(1)} %get-tuple-element.10.refs_0_, bf16[1,128,1024]{2,1,0:T(8,128)(2,1)S(1)} %get-tuple-element.11.refs_1_, ...), custom_call_target="tpu_custom_call" | custom-call | tf_op jit(solution)/shard_map/pallas_call | solution.py:1095
